TPU v7x, 32 devices: a whole 2x2x4 slice. The times are simulated.
32 devices in a mesh: sp: 8 (over z, x), tp: 4 (over y, core).
Axes of the slice: x: 2, y: 2, z: 4, core: 2. Of those that a mesh axis runs over, the one named last changes fastest.
Arguments:
- query_proj: bfloat16 [4096, 1024], P('sp', 'tp'), may hold values from -6 to 6
- projected_keys: bfloat16 [4096, 512], P('sp', 'tp'), may hold values from -6 to 6
- projected_values: bfloat16 [4096, 512], P('sp', 'tp'), may hold values from -6 to 6
- residual: bfloat16 [4096, 2048], P(('sp', 'tp')), may hold values from -6 to 6
- out_weight: bfloat16 [1024, 2048], replicated, may hold values from -0.1875 to 0.1875
- mix_gain: float32 [2048], replicated, may hold values from 0.1 to 1.9
- norm_gain: float32 [2048], replicated, may hold values from 0.1 to 1.9
- route_expert: int32 [4096, 2], P(('sp', 'tp')), may hold values from 0 to 31, all different within a row; in each aligned block of 128 rows (0 to 127, 128 to 255, ...) at most 16 rows name the same one
- route_weight: float32 [4096, 2], P(('sp', 'tp')), may hold values from 0.2 to 1
- expert_gate: bfloat16 [32, 2048, 1024], P(('sp', 'tp')), may hold values from -0.125 to 0.125
- expert_up: bfloat16 [32, 2048, 1024], P(('sp', 'tp')), may hold values from -0.125 to 0.125
- expert_down: bfloat16 [32, 1024, 2048], P(('sp', 'tp')), may hold values from -0.1875 to 0.1875
Outputs:
- output: bfloat16 [4096, 2048], P(('sp', 'tp'))
Inputs may be any that keep to these rules, and one draw needn't show every extreme that they name: `route_expert`: each row names 2 different experts. The rows of one device (aligned blocks of 128 rows) name any one expert at most 16 times, and in some blocks some expert is named exactly 16 times.
All inputs are finite; a program needn't handle non-finite values.
Results may differ from a plain program's by a relative error of at most 0.015.
Values may be sent and summed in bfloat16 or wider, within the bound.
A program may use at most 128 MiB of HBM per device.

v0:
```python
import functools
import math

import jax
import jax.numpy as jnp
from jax import lax
from jax.experimental import pallas as pl
from jax.experimental.pallas import tpu as pltpu
from jax.sharding import PartitionSpec as P

D = 2048
HEAD_SIZE = 64
GRID_W = 64


epsilon = 1e-06
base_theta = 10000.0


def unit_length_rows(values):
    values = values.astype(jnp.float32)
    return values * lax.rsqrt(jnp.mean(values * values, axis=-1, keepdims=True) + epsilon)


MESH = pl.DeviceIdType.MESH
LANES = 2 * HEAD_SIZE


def ring_step(sp, delta, n, nz, nx):
    z, x = sp // nx, sp % nx
    place = x * nz + z + (x % 2) * (nz - 1 - 2 * z)
    place = (place + delta + n) % n
    x = place // nz
    z = place % nz
    z = z + (x % 2) * (nz - 1 - 2 * z)
    return z * nx + x


def attend_kernel(
    n, nz, nx, ntp, group,
    q_ref, k_ref, v_ref, cos_ref, sin_ref, swap_ref, ones_ref,
    out_ref,
    qs, acc, fb, bb, att, rx,
    send_f, recv_f, send_b, recv_b, send_t, recv_t,
):
    sp = lax.axis_index("sp")
    tp = lax.axis_index("tp")
    toks = q_ref.shape[0]
    heads = q_ref.shape[1] // HEAD_SIZE
    half = toks // 2
    steps = n - 1
    nxt = ring_step(sp, 1, n, nz, nx)
    prv = ring_step(sp, -1, n, nz, nx)

    barrier = pltpu.get_barrier_semaphore()
    for other in (nxt, prv):
        pl.semaphore_signal(barrier, inc=1, device_id=(other, tp), device_id_type=MESH)
    for d in range(1, ntp):
        pl.semaphore_signal(
            barrier, inc=1, device_id=(sp, (tp + d) % ntp), device_id_type=MESH
        )

    cos = cos_ref[...]
    sin = sin_ref[...]
    low = lax.broadcasted_iota(jnp.int32, (toks, LANES), 1) < HEAD_SIZE

    def prepare(block):
        wide = block.astype(jnp.float32)
        square = wide * wide
        hi = square.astype(jnp.bfloat16)
        lo = (square - hi.astype(jnp.float32)).astype(jnp.bfloat16)
        mean = jnp.dot(hi, ones_ref[...], preferred_element_type=jnp.float32) + jnp.dot(
            lo, ones_ref[...], preferred_element_type=jnp.float32
        )
        partner = jnp.dot(block, swap_ref[...], preferred_element_type=jnp.float32)
        return (wide * cos + partner * sin) * lax.rsqrt(mean + epsilon)

    keys = prepare(k_ref[...]).astype(jnp.bfloat16)
    vals = v_ref[...]
    for c in range(2):
        rows = slice(c * half, (c + 1) * half)
        fb[c, 0] = keys[rows]
        fb[c, 1] = vals[rows]
        bb[1 - c, 0] = keys[rows]
        bb[1 - c, 1] = vals[rows]

    def forward(i):
        return pltpu.make_async_remote_copy(
            src_ref=fb.at[i], dst_ref=fb.at[i + 2],
            send_sem=send_f.at[i], recv_sem=recv_f.at[i],
            device_id=(nxt, tp), device_id_type=MESH,
        )

    def backward(i):
        return pltpu.make_async_remote_copy(
            src_ref=bb.at[i], dst_ref=bb.at[i + 2],
            send_sem=send_b.at[i], recv_sem=recv_b.at[i],
            device_id=(prv, tp), device_id_type=MESH,
        )

    pl.semaphore_wait(barrier, 2 + ntp - 1)
    for i in range(2):
        forward(i).start()
        backward(i).start()

    scale = HEAD_SIZE ** (-0.5)
    for t in range(heads // 2):
        ready = prepare(q_ref[:, t * LANES : (t + 1) * LANES]) * scale
        for h in (2 * t, 2 * t + 1):
            side = (h // group) % 2
            lined = ready if h % 2 == side else pltpu.roll(ready, HEAD_SIZE, 1)
            keep = low if side == 0 else jnp.logical_not(low)
            qs[h * toks : (h + 1) * toks] = jnp.where(keep, lined, 0.0).astype(jnp.bfloat16)
    acc[...] = jnp.zeros_like(acc)
    tile = math.gcd(toks, 256)
    vlow = lax.broadcasted_iota(jnp.int32, (toks, LANES), 1) < HEAD_SIZE

    def one_step(j, carry):
        at = j + jnp.minimum(j, 1)

        @pl.when(j > 0)
        def _():
            forward(j - 1).wait_recv()
            backward(j - 1).wait_recv()

        @pl.when(jnp.logical_and(j > 0, j + 1 < steps))
        def _():
            forward(j + 1).start()
            backward(j + 1).start()

        kk = jnp.concatenate([fb[at, 0], bb[at, 0]], axis=0)
        vv = jnp.concatenate([fb[at, 1], bb[at, 1]], axis=0).astype(jnp.float32)
        sided = (
            jnp.where(vlow, vv, 1.0).astype(jnp.bfloat16),
            jnp.where(vlow, 1.0, vv).astype(jnp.bfloat16),
        )
        for h in range(heads):
            for r in range(toks // tile):
                rows = slice(h * toks + r * tile, h * toks + (r + 1) * tile)
                scores = lax.dot_general(
                    qs[rows], kk, (((1,), (1,)), ((), ())),
                    preferred_element_type=jnp.float32,
                )
                weights = jnp.exp(scores).astype(jnp.bfloat16)
                acc[rows] += jnp.dot(
                    weights, sided[(h // group) % 2], preferred_element_type=jnp.float32
                )
        return carry

    lax.fori_loop(0, steps + 1, one_step, 0)

    share = toks // ntp
    for t in range(heads // 2):
        parts = []
        for h in (2 * t, 2 * t + 1):
            mine = acc[h * toks : (h + 1) * toks]
            turned = pltpu.roll(mine, HEAD_SIZE, 1)
            parts.append(mine / turned if h % 2 == (h // group) % 2 else turned / mine)
        done = jnp.where(low, parts[0], parts[1]).astype(jnp.bfloat16)
        for p in range(ntp):
            att[p, :, t * LANES : (t + 1) * LANES] = done[p * share : (p + 1) * share]

    def across(d):
        to = (tp + d) % ntp
        return pltpu.make_async_remote_copy(
            src_ref=att.at[to], dst_ref=rx.at[tp],
            send_sem=send_t.at[d], recv_sem=recv_t.at[d],
            device_id=(sp, to), device_id_type=MESH,
        )

    for d in range(1, ntp):
        across(d).start()
    rx[tp] = att[tp]
    for i in range(steps):
        forward(i).wait_send()
        backward(i).wait_send()
    for d in range(1, ntp):
        across(d).wait_recv()
    width = q_ref.shape[1]
    for p in range(ntp):
        out_ref[:, p * width : (p + 1) * width] = rx[p]
    for d in range(1, ntp):
        across(d).wait_send()


def ring_sizes(mesh, n):
    try:
        coords = [tuple(d.coords) for d in mesh.devices[:, 0]]
        nz = len({c[2] for c in coords})
        nx = len({c[0] for c in coords})
        if nz * nx == n and nz > 1:
            return nz, nx
    except Exception:
        pass
    return n, 1


def attend(mesh, query_proj, projected_keys, projected_values):
    n, ntp = mesh.shape["sp"], mesh.shape["tp"]
    nz, nx = ring_sizes(mesh, n)
    toks, width = query_proj.shape
    heads = width // HEAD_SIZE
    group = heads // (projected_keys.shape[1] // HEAD_SIZE)
    spare = LANES - projected_keys.shape[1]
    if spare:
        projected_keys = jnp.pad(projected_keys, ((0, 0), (0, spare)))
        projected_values = jnp.pad(projected_values, ((0, 0), (0, spare)))
    quarter = HEAD_SIZE // 4
    places = lax.axis_index("sp") * toks + jnp.arange(toks, dtype=jnp.int32)
    frequency = base_theta ** (-jnp.arange(quarter, dtype=jnp.float32) / quarter)
    lane = jnp.arange(LANES, dtype=jnp.int32)
    on_row = (lane % HEAD_SIZE) < 2 * quarter
    spot = jnp.where(on_row[None, :], (places // GRID_W)[:, None], (places % GRID_W)[:, None])
    angle = spot.astype(jnp.float32) * jnp.tile(frequency, LANES // quarter)[None, :]
    first = (lane // quarter) % 2 == 0
    source = jnp.where(first, lane + quarter, lane - quarter)
    swap = jnp.where(
        lane[:, None] == source[None, :], jnp.where(first, -1.0, 1.0)[None, :], 0.0
    ).astype(jnp.bfloat16)
    ones = jnp.where(
        lane[:, None] // HEAD_SIZE == lane[None, :] // HEAD_SIZE, 1.0 / HEAD_SIZE, 0.0
    ).astype(jnp.bfloat16)
    share = toks // ntp
    dma = pltpu.SemaphoreType.DMA
    return pl.pallas_call(
        functools.partial(attend_kernel, n, nz, nx, ntp, group),
        out_shape=jax.ShapeDtypeStruct((share, ntp * width), jnp.bfloat16),
        in_specs=[pl.BlockSpec(memory_space=pltpu.VMEM)] * 7,
        out_specs=pl.BlockSpec(memory_space=pltpu.VMEM),
        scratch_shapes=[
            pltpu.VMEM((heads * toks, LANES), jnp.bfloat16),
            pltpu.VMEM((heads * toks, LANES), jnp.float32),
            pltpu.VMEM((n + 1, 2, toks // 2, LANES), jnp.bfloat16),
            pltpu.VMEM((n + 1, 2, toks // 2, LANES), jnp.bfloat16),
            pltpu.VMEM((ntp, share, width), jnp.bfloat16),
            pltpu.VMEM((ntp, share, width), jnp.bfloat16),
            dma((n - 1,)), dma((n - 1,)), dma((n - 1,)), dma((n - 1,)),
            dma((ntp,)), dma((ntp,)),
        ],
        compiler_params=pltpu.CompilerParams(
            collective_id=0, has_side_effects=True, vmem_limit_bytes=40 << 20
        ),
        name="attend",
    )(query_proj, projected_keys, projected_values, jnp.cos(angle), jnp.sin(angle), swap, ones)


def moe_kernel(
    count, ntp, cap,
    tx, stream, pick, share_w, gate_hbm, up_hbm, down_hbm,
    out_ref,
    rx, res, ret, act, gate, up, down,
    send_o, recv_o, send_r, recv_r, wsem,
):
    me = lax.axis_index("sp") * ntp + lax.axis_index("tp")
    per = count // 4
    order = (2, 1, 3, 0)

    def device(offset):
        other = (me + offset + count) % count
        return (other // ntp, other % ntp)

    def block(d):
        return pl.ds(pl.multiple_of(d * cap, cap), cap)

    def dispatch(d):
        return pltpu.make_async_remote_copy(
            src_ref=tx.at[block(d)], dst_ref=rx.at[block(d)],
            send_sem=send_o.at[d], recv_sem=recv_o.at[d],
            device_id=device(d), device_id_type=MESH,
        )

    def answer(d):
        return pltpu.make_async_remote_copy(
            src_ref=res.at[block(d)], dst_ref=ret.at[block(d)],
            send_sem=send_r.at[d], recv_sem=recv_r.at[d],
            device_id=device(-d), device_id_type=MESH,
        )

    def each(first, last, action):
        def body(d, carry):
            action(d)
            return carry

        lax.fori_loop(max(first, 1), last, body, 0)

    barrier = pltpu.get_barrier_semaphore()
    each(1, count, lambda d: pl.semaphore_signal(
        barrier, inc=1, device_id=device(d), device_id_type=MESH
    ))
    loads = [
        pltpu.make_async_copy(gate_hbm.at[0], gate, wsem.at[0]),
        pltpu.make_async_copy(up_hbm.at[0], up, wsem.at[1]),
        pltpu.make_async_copy(down_hbm.at[0], down, wsem.at[2]),
    ]
    pl.semaphore_wait(barrier, count - 1)
    for g in order:
        each(g * per, (g + 1) * per, lambda d: dispatch(d).start())
    for load in loads:
        load.start()
    rx[0:cap] = tx[0:cap]

    def columns(total, body):
        tile = math.gcd(total, 256)

        def one(c, carry):
            body(pl.ds(pl.multiple_of(c * tile, tile), tile))
            return carry

        lax.fori_loop(0, total // tile, one, 0)

    for number, g in enumerate(order):
        each(g * per, (g + 1) * per, lambda d: dispatch(d).wait_recv())
        if number == 0:
            for load in loads:
                load.wait()
        rows = slice(g * per * cap, (g + 1) * per * cap)

        def hidden(cols):
            taken = rx[rows]
            pre = jnp.dot(taken, gate[:, cols], preferred_element_type=jnp.float32)
            lift = jnp.dot(taken, up[:, cols], preferred_element_type=jnp.float32)
            act[:, cols] = (pre / (1.0 + jnp.exp(-pre)) * lift).astype(jnp.bfloat16)

        def project(cols):
            res[rows, cols] = jnp.dot(
                act[...], down[:, cols], preferred_element_type=jnp.float32
            ).astype(jnp.bfloat16)

        columns(gate.shape[1], hidden)
        columns(down.shape[1], project)
        each(g * per, (g + 1) * per, lambda d: answer(d).start())
    ret[0:cap] = res[0:cap]
    each(1, count, lambda d: answer(d).wait_recv())

    def combine(cols):
        total = jnp.zeros((out_ref.shape[0], math.gcd(out_ref.shape[1], 256)), jnp.float32)
        for k in range(pick.shape[0]):
            total += share_w[:, k : k + 1] * jnp.dot(
                pick[k], ret[:, cols], preferred_element_type=jnp.float32
            )
        out_ref[:, cols] = (stream[:, cols].astype(jnp.float32) + total).astype(jnp.bfloat16)

    columns(out_ref.shape[1], combine)
    each(1, count, lambda d: dispatch(d).wait_send())
    each(1, count, lambda d: answer(d).wait_send())


def moe(mesh, cap, outgoing, stream, pick, share_w, expert_gate, expert_up, expert_down):
    ntp = mesh.shape["tp"]
    count = mesh.shape["sp"] * ntp
    width = outgoing.shape[1]
    ff = expert_gate.shape[2]
    dma = pltpu.SemaphoreType.DMA
    low = jnp.bfloat16
    return pl.pallas_call(
        functools.partial(moe_kernel, count, ntp, cap),
        out_shape=jax.ShapeDtypeStruct(stream.shape, low),
        in_specs=[pl.BlockSpec(memory_space=pltpu.VMEM)] * 4
        + [pl.BlockSpec(memory_space=pl.ANY)] * 3,
        out_specs=pl.BlockSpec(memory_space=pltpu.VMEM),
        scratch_shapes=[
            pltpu.VMEM((count * cap, width), low),
            pltpu.VMEM((count * cap, width), low),
            pltpu.VMEM((count * cap, width), low),
            pltpu.VMEM((count // 4 * cap, ff), low),
            pltpu.VMEM((width, ff), low),
            pltpu.VMEM((width, ff), low),
            pltpu.VMEM((ff, width), low),
            dma((count,)), dma((count,)), dma((count,)), dma((count,)), dma((3,)),
        ],
        compiler_params=pltpu.CompilerParams(
            collective_id=1, has_side_effects=True, vmem_limit_bytes=60 << 20
        ),
        name="moe",
    )(outgoing, stream, pick, share_w, expert_gate, expert_up, expert_down)


def local(
    mesh,
    query_proj,
    projected_keys,
    projected_values,
    residual,
    out_weight,
    mix_gain,
    norm_gain,
    route_expert,
    route_weight,
    expert_gate,
    expert_up,
    expert_down,
):
    by_token = attend(mesh, query_proj, projected_keys, projected_values)
    mixed = jnp.dot(by_token, out_weight, preferred_element_type=jnp.float32)
    stream = (residual.astype(jnp.float32) + unit_length_rows(mixed) * mix_gain).astype(
        jnp.bfloat16
    )
    normed = (unit_length_rows(stream) * norm_gain).astype(jnp.bfloat16)
    row_count = normed.shape[0]
    top_count = route_expert.shape[1]
    experts = lax.axis_size("sp") * lax.axis_size("tp")
    capacity = -(-max(2, 2 * top_count * row_count // experts) // 16) * 16
    flat_expert = route_expert.reshape(-1)
    onehot = (flat_expert[:, None] == jnp.arange(experts, dtype=jnp.int32)[None, :]).astype(
        jnp.int32
    )
    earlier = jnp.cumsum(onehot, axis=0) - onehot
    slot_rank = jnp.sum(earlier * onehot, axis=1)
    me = lax.axis_index("sp") * lax.axis_size("tp") + lax.axis_index("tp")
    target = ((flat_expert - me + experts) % experts) * capacity + slot_rank
    placing = jnp.arange(experts * capacity, dtype=jnp.int32)[:, None] == target[None, :]
    placing = jnp.any(placing.reshape(experts * capacity, row_count, top_count), axis=2).astype(
        jnp.bfloat16
    )
    outgoing = jnp.dot(placing, normed, preferred_element_type=jnp.float32).astype(jnp.bfloat16)
    places = jnp.arange(experts * capacity, dtype=jnp.int32)
    pick = target.reshape(row_count, top_count).T[:, :, None] == places
    return moe(
        mesh, capacity, outgoing, stream, pick.astype(jnp.bfloat16), route_weight,
        expert_gate, expert_up, expert_down,
    )


def solution(mesh):
    return jax.shard_map(
        functools.partial(local, mesh),
        mesh=mesh,
        in_specs=(
            P("sp", "tp"),
            P("sp", "tp"),
            P("sp", "tp"),
            P(("sp", "tp"), None),
            P(),
            P(),
            P(),
            P(("sp", "tp"), None),
            P(("sp", "tp"), None),
            P(("sp", "tp"), None, None),
            P(("sp", "tp"), None, None),
            P(("sp", "tp"), None, None),
        ),
        out_specs=P(("sp", "tp"), None),
        check_vma=False,
    )
```

profile of v0, /device:TPU:16, one launch (start us, length us, event | category | flops | bytes accessed | tf_op | source)
XLA Modules:
  0.0 151.5 jit_solution(69884216899318785)
XLA Ops:
  0.1 0.1 mul.73
  0.2 0.0 copy-start.4
  0.2 0.0 copy-start.5
  0.2 0.1 select_convert_fusion.ones_ref
  0.3 0.8 copy.40
  1.1 0.1 eq.101
  1.3 0.1 eq.97
  1.4 0.6 reduce-window.6
  2.0 0.2 slice_reduce_fusion
  2.2 0.1 fusion.12
  2.3 0.1 reduce_sum.30
  2.5 0.1 copy.43
  2.6 0.7 fusion.18
  3.3 0.1 fusion.6
  3.3 1.4 copy.44.share_w
  4.7 0.8 fusion.7.pick
  5.5 1.0 fusion.8
  6.6 0.0 copy-start
  6.6 0.9 copy-done
  7.5 0.0 copy-start.1
  7.5 0.9 copy-done.1
  8.4 0.0 copy-start.2
  8.4 0.9 copy-done.2
  9.3 0.0 copy-start.6
  9.3 29.7 %attend.1 = bf16[128,1024]{1,0:T(8,128)(2,1)S(1)} custom-call(bf16[512,256]{1,0:T(8,128)(2,1)S(1)} %copy-done, bf16[512,128]{1,0:T(8,128)(2,1)S(1)} %copy-done.1, bf16[512,128]{1,0:T(8,128)(2,1)S(1)} %copy-done.2, f32[512,128]{1,0:T(8,128)S(1)} %get-tuple-element.8.cos_ref, f32[512,128]{1,0:T(8,128)S(1)} %get-tuple-element.7.sin_ref, ...), custom_call_target="tpu_custom_call" | custom-call | tf_op jit(solution)/shard_map/attend/pallas_call | solution.py:225
  39.1 3.0 %multiply_reduce_fusion = (f32[128]{0:T(128)S(1)}, f32[128,2048]{1,0:T(8,128)S(1)}) fusion(bf16[128,1024]{1,0:T(8,128)(2,1)S(1)} %attend.1, bf16[1024,2048]{1,0:T(8,128)(2,1)} %param.16), kind=kOutput, calls=%fused_computation.7 | convolution fusion | flops 537395072 | bytes 5505536 | tf_op jit(solution)/shard_map/dot_general | solution.py:394
  42.1 0.0 copy-done.4
  42.1 0.0 copy-done.5
  42.1 0.4 fusion
  42.5 0.0 copy-start.3
  42.5 0.0 copy-done.6
  42.5 2.1 %convolution_convert_fusion.tx = bf16[512,2048]{1,0:T(8,128)(2,1)} fusion(pred[512,128]{1,0:T(8,128)(4,1)S(1)} %fusion.6, bf16[128,2048]{1,0:T(8,128)(2,1)S(1)} %get-tuple-element.6.stream, f32[2048]{0:T(1024)S(1)} %copy-done.6, f32[128]{0:T(128)S(1)} %add_rsqrt_fusion), kind=kOutput, calls=%fused_computation | convolution fusion | flops 270532608 | bytes 2695680 | tf_op jit(solution)/shard_map/dot_general | solution.py:415
  44.6 0.0 copy-done.3
  44.6 104.9 %moe.1 = bf16[128,2048]{1,0:T(8,128)(2,1)} custom-call(bf16[512,2048]{1,0:T(8,128)(2,1)} %convolution_convert_fusion.tx, bf16[128,2048]{1,0:T(8,128)(2,1)} %copy-done.3, bf16[2,128,512]{2,1,0:T(8,128)(2,1)} %fusion.7.pick, f32[128,2]{1,0:T(8,128)} %copy.44.share_w, bf16[1,2048,1024]{2,1,0:T(8,128)(2,1)} %gate_hbm.1, bf16[1,2048,1024]{2,1,0:T(8,128)(2,1)} %up_hbm.1, ...), custom_call_target="tpu_custom_call" | custom-call | tf_op jit(solution)/shard_map/moe/pallas_call | solution.py:355
  149.6 1.9 %copy.48 = bf16[128,2048]{1,0:T(8,128)(2,1)} copy(bf16[128,2048]{1,0:T(8,128)(2,1)} %moe.1) | data formatting | bytes 1048576
  (13 shorter events, 0.1 us)
Async XLA Ops:
  0.2 41.9 %copy-start.4 = (bf16[128,2048]{1,0:T(8,128)(2,1)S(1)}, bf16[128,2048]{1,0:T(8,128)(2,1)}, u32[]{:S(2)}) copy-start(bf16[128,2048]{1,0:T(8,128)(2,1)} %param.15) | copy-start | bytes 1572868
  0.2 41.9 %copy-start.5 = (f32[2048]{0:T(1024)S(1)}, f32[2048]{0:T(1024)}, u32[]{:S(2)}) copy-start(f32[2048]{0:T(1024)} %param.17) | copy-start | bytes 24580
  6.6 1.0 copy-start
  7.5 0.9 copy-start.1
  8.4 0.9 copy-start.2
  9.3 33.2 %copy-start.6 = (f32[2048]{0:T(1024)S(1)}, f32[2048]{0:T(1024)}, u32[]{:S(2)}) copy-start(f32[2048]{0:T(1024)} %param.18) | copy-start | bytes 24580
  42.5 2.2 %copy-start.3 = (bf16[128,2048]{1,0:T(8,128)(2,1)}, bf16[128,2048]{1,0:T(8,128)(2,1)S(1)}, u32[]{:S(2)}) copy-start(bf16[128,2048]{1,0:T(8,128)(2,1)S(1)} %get-tuple-element.6.stream) | copy-start | bytes 1572868
where the time goes:
time: 152 us; the launch traced here: 151 us
  Pallas kernels  135 us (89%)
  local copies, waits for them, and re-layouts  7.62 us (5%)
  matrix products  5.13 us (3%)
  other arithmetic  3.86 us (3%)
    pallas_call x1, Pallas kernels, moe(): pl.pallas_call(functools.partial(moe_kernel, count, ntp, cap), out_shape=...  105 us
    pallas_call x1, Pallas kernels, attend(): pl.pallas_call(functools.partial(attend_kernel, n, nz, nx, ntp, group), o...  29.7 us
    unnamed x17, local copies, waits for them, and re-layouts  6.88 us

commit v1 on v0

--- a/solution.py
+++ b/solution.py
@@ -245,134 +245,393 @@
 
 
 def moe_kernel(
-    count, ntp, cap,
-    tx, stream, pick, share_w, gate_hbm, up_hbm, down_hbm,
+    nz, nx, ntp, cap, cuts,
+    normed, stream, route, share_w, gate_hbm, up_hbm, down_hbm,
     out_ref,
-    rx, res, ret, act, gate, up, down,
-    send_o, recv_o, send_r, recv_r, wsem,
+    info, blk, tx, rx, res, ret, inc, part, snd, place, weigh, act, gate, up, down,
+    send_i, recv_i, send_u, send_d, recv_z, send_o, recv_o, send_r, recv_r, send_p, recv_p, wsem,
 ):
-    me = lax.axis_index("sp") * ntp + lax.axis_index("tp")
-    per = count // 4
-    order = (2, 1, 3, 0)
-
-    def device(offset):
-        other = (me + offset + count) % count
-        return (other // ntp, other % ntp)
-
-    def block(d):
-        return pl.ds(pl.multiple_of(d * cap, cap), cap)
-
-    def dispatch(d):
+    sp = lax.axis_index("sp")
+    tp = lax.axis_index("tp")
+    z = sp // nx
+    p = (sp % nx) * ntp + tp
+    plane = nx * ntp
+    slots = plane * cap
+    toks, width = normed.shape
+    wide = width // cuts
+    others = (plane - 1) * cap
+
+    def device(zz, pp):
+        return (zz * nx + pp // ntp, pp % ntp)
+
+    def cols(c):
+        return pl.ds(pl.multiple_of(c * wide, wide), wide)
+
+    def rows(pp):
+        return pl.ds(pl.multiple_of(pp * cap, cap), cap)
+
+    def remote(src, dst, send, recv, to):
         return pltpu.make_async_remote_copy(
-            src_ref=tx.at[block(d)], dst_ref=rx.at[block(d)],
-            send_sem=send_o.at[d], recv_sem=recv_o.at[d],
-            device_id=device(d), device_id_type=MESH,
-        )
-
-    def answer(d):
-        return pltpu.make_async_remote_copy(
-            src_ref=res.at[block(d)], dst_ref=ret.at[block(d)],
-            send_sem=send_r.at[d], recv_sem=recv_r.at[d],
-            device_id=device(-d), device_id_type=MESH,
-        )
-
-    def each(first, last, action):
-        def body(d, carry):
-            action(d)
+            src_ref=src, dst_ref=dst, send_sem=send, recv_sem=recv,
+            device_id=to, device_id_type=MESH,
+        )
+
+    def loop(first, last, action):
+        def body(i, carry):
+            action(i)
             return carry
 
-        lax.fori_loop(max(first, 1), last, body, 0)
+        lax.fori_loop(first, last, body, 0)
+
+    def facts(k):
+        to = (z + k) % nz
+        return remote(info.at[z], info.at[z], send_i.at[k], recv_i.at[k], device(to, p))
+
+    def facts_in(k):
+        zz = (z - k + nz) % nz
+        return remote(info.at[zz], info.at[zz], send_i.at[k], recv_i.at[k], device(zz, p))
+
+    def own_hop(c, up_way):
+        send = send_u if up_way else send_d
+        return remote(
+            normed.at[:, cols(c)], blk.at[z, :, cols(c)], send.at[z, c], recv_z.at[z, c],
+            device(z + 1 if up_way else z - 1, p),
+        )
+
+    def hop(zz, c, up_way):
+        send = send_u if up_way else send_d
+        return remote(
+            blk.at[zz, :, cols(c)], blk.at[zz, :, cols(c)], send.at[zz, c], recv_z.at[zz, c],
+            device(z + 1 if up_way else z - 1, p),
+        )
+
+    def dispatch(zz, c, q):
+        pp = (p + q) % plane
+        return remote(
+            tx.at[zz, rows(pp), cols(c)], rx.at[zz, rows(p), cols(c)],
+            send_o.at[zz], recv_o.at[zz], device(z, pp),
+        )
+
+    def dispatch_all(zz):
+        some = pl.ds(0, others)
+        return remote(tx.at[zz, some], rx.at[zz, some], send_o.at[zz], recv_o.at[zz], device(z, p))
+
+    def answer(zz, c, q):
+        pp = (p + q) % plane
+        return remote(
+            res.at[zz, rows(pp), cols(c)], ret.at[zz, rows(p), cols(c)],
+            send_r.at[zz], recv_r.at[zz, c], device(z, pp),
+        )
+
+    def answer_in(zz, c):
+        some = pl.ds(0, others)
+        return remote(
+            res.at[zz, some, cols(c)], ret.at[zz, some, cols(c)],
+            send_r.at[zz], recv_r.at[zz, c], device(z, p),
+        )
+
+    def answer_sent(zz):
+        some = pl.ds(0, others)
+        return remote(res.at[zz, some], ret.at[zz, some], send_r.at[zz], recv_r.at[zz, 0], device(z, p))
+
+    def partial_out(zz, c):
+        step = jnp.where(zz > z, 1, -1)
+        slot = jnp.where(zz == z + 1, nz, zz)
+        return remote(
+            snd.at[zz, :, cols(c)], inc.at[slot, :, cols(c)],
+            send_p.at[zz, c], recv_p.at[slot, c], device(z + step, p),
+        )
+
+    def partial_in(slot, c):
+        return remote(
+            snd.at[0, :, cols(c)], inc.at[slot, :, cols(c)],
+            send_p.at[0, c], recv_p.at[slot, c], device(z, p),
+        )
 
     barrier = pltpu.get_barrier_semaphore()
-    each(1, count, lambda d: pl.semaphore_signal(
-        barrier, inc=1, device_id=device(d), device_id_type=MESH
-    ))
+    for k in range(1, nz):
+        pl.semaphore_signal(barrier, inc=1, device_id=device((z + k) % nz, p), device_id_type=MESH)
+    for q in range(1, plane):
+        pl.semaphore_signal(barrier, inc=1, device_id=device(z, (p + q) % plane), device_id_type=MESH)
     loads = [
         pltpu.make_async_copy(gate_hbm.at[0], gate, wsem.at[0]),
         pltpu.make_async_copy(up_hbm.at[0], up, wsem.at[1]),
         pltpu.make_async_copy(down_hbm.at[0], down, wsem.at[2]),
     ]
-    pl.semaphore_wait(barrier, count - 1)
-    for g in order:
-        each(g * per, (g + 1) * per, lambda d: dispatch(d).start())
     for load in loads:
         load.start()
-    rx[0:cap] = tx[0:cap]
-
-    def columns(total, body):
+
+    experts = nz * plane
+    at_expert = lax.broadcasted_iota(jnp.int32, (experts, toks), 0)
+    named = [at_expert == route[k : k + 1, :] for k in range(2)]
+    count = (named[0].astype(jnp.float32) + named[1].astype(jnp.float32)).astype(jnp.bfloat16)
+    before = (
+        lax.broadcasted_iota(jnp.int32, (toks, toks), 0)
+        < lax.broadcasted_iota(jnp.int32, (toks, toks), 1)
+    ).astype(jnp.float32).astype(jnp.bfloat16)
+    earlier = jnp.dot(count, before, preferred_element_type=jnp.float32)
+    lines = []
+    for k in range(2):
+        rank = jnp.sum(jnp.where(named[k], earlier, 0.0), axis=0, keepdims=True)
+        lines.append(route[k : k + 1, :].astype(jnp.float32) * float(cap) + rank)
+    info[z] = jnp.concatenate(
+        lines + [share_w[...], jnp.zeros((4, toks), jnp.float32)], axis=0
+    )
+
+    pl.semaphore_wait(barrier, nz - 1 + plane - 1)
+    for k in range(1, nz):
+        facts(k).start()
+
+    @pl.when(z + 1 < nz)
+    def _():
+        loop(0, cuts, lambda c: own_hop(c, True).start())
+
+    @pl.when(z > 0)
+    def _():
+        loop(0, cuts, lambda c: own_hop(c, False).start())
+
+    def learn(zz):
+        known = info[zz]
+        spot = (
+            lax.broadcasted_iota(jnp.int32, (slots, toks), 0) + z * slots
+        ).astype(jnp.float32)
+        first = spot == known[0:1, :]
+        second = spot == known[1:2, :]
+        place[zz] = jnp.where(first | second, 1.0, 0.0).astype(jnp.bfloat16)
+        amount = jnp.where(first, known[2:3, :], 0.0) + jnp.where(second, known[3:4, :], 0.0)
+        turned = amount.T
+        hi = turned.astype(jnp.bfloat16)
+        weigh[zz, :, 0:slots] = hi
+        weigh[zz, :, slots : 2 * slots] = (turned - hi.astype(jnp.float32)).astype(jnp.bfloat16)
+
+    def pack(zz, c, block):
+        packed = jnp.dot(
+            place[zz], block, preferred_element_type=jnp.float32
+        ).astype(jnp.bfloat16)
+        tx[zz, :, cols(c)] = packed
+        for q in range(1, plane):
+            dispatch(zz, c, q).start()
+        rx[zz, rows(p), cols(c)] = tx[zz, rows(p), cols(c)]
+
+    def columns(first, total, body):
         tile = math.gcd(total, 256)
 
         def one(c, carry):
-            body(pl.ds(pl.multiple_of(c * tile, tile), tile))
+            body(pl.ds(pl.multiple_of(first + c * tile, tile), tile))
             return carry
 
         lax.fori_loop(0, total // tile, one, 0)
 
-    for number, g in enumerate(order):
-        each(g * per, (g + 1) * per, lambda d: dispatch(d).wait_recv())
-        if number == 0:
-            for load in loads:
-                load.wait()
-        rows = slice(g * per * cap, (g + 1) * per * cap)
-
-        def hidden(cols):
-            taken = rx[rows]
-            pre = jnp.dot(taken, gate[:, cols], preferred_element_type=jnp.float32)
-            lift = jnp.dot(taken, up[:, cols], preferred_element_type=jnp.float32)
-            act[:, cols] = (pre / (1.0 + jnp.exp(-pre)) * lift).astype(jnp.bfloat16)
-
-        def project(cols):
-            res[rows, cols] = jnp.dot(
-                act[...], down[:, cols], preferred_element_type=jnp.float32
+    def expert(zz):
+        dispatch_all(zz).wait_recv()
+
+        def hidden(at):
+            taken = rx[zz]
+            pre = jnp.dot(taken, gate[:, at], preferred_element_type=jnp.float32)
+            lift = jnp.dot(taken, up[:, at], preferred_element_type=jnp.float32)
+            act[:, at] = (pre / (1.0 + jnp.exp(-pre)) * lift).astype(jnp.bfloat16)
+
+        def project(at):
+            res[zz, :, at] = jnp.dot(
+                act[...], down[:, at], preferred_element_type=jnp.float32
             ).astype(jnp.bfloat16)
 
-        columns(gate.shape[1], hidden)
-        columns(down.shape[1], project)
-        each(g * per, (g + 1) * per, lambda d: answer(d).start())
-    ret[0:cap] = res[0:cap]
-    each(1, count, lambda d: answer(d).wait_recv())
-
-    def combine(cols):
-        total = jnp.zeros((out_ref.shape[0], math.gcd(out_ref.shape[1], 256)), jnp.float32)
-        for k in range(pick.shape[0]):
-            total += share_w[:, k : k + 1] * jnp.dot(
-                pick[k], ret[:, cols], preferred_element_type=jnp.float32
+        columns(0, gate.shape[1], hidden)
+
+        def send(c):
+            columns(c * wide, wide, project)
+            for q in range(1, plane):
+                answer(zz, c, q).start()
+            ret[zz, rows(p), cols(c)] = res[zz, rows(p), cols(c)]
+
+        loop(0, cuts, send)
+
+    def gather(zz):
+        last = jnp.logical_and(
+            zz != z,
+            jnp.logical_or(
+                jnp.logical_and(zz > z, z == 0), jnp.logical_and(zz < z, z == nz - 1)
+            ),
+        )
+
+        def one(c):
+            answer_in(zz, c).wait_recv()
+            back = ret[zz, :, cols(c)]
+            total = jnp.dot(
+                weigh[zz, :, 0:slots], back, preferred_element_type=jnp.float32
+            ) + jnp.dot(
+                weigh[zz, :, slots : 2 * slots], back, preferred_element_type=jnp.float32
             )
-        out_ref[:, cols] = (stream[:, cols].astype(jnp.float32) + total).astype(jnp.bfloat16)
-
-    columns(out_ref.shape[1], combine)
-    each(1, count, lambda d: dispatch(d).wait_send())
-    each(1, count, lambda d: answer(d).wait_send())
-
-
-def moe(mesh, cap, outgoing, stream, pick, share_w, expert_gate, expert_up, expert_down):
+            part[zz, :, cols(c)] = total
+
+            @pl.when(last)
+            def _():
+                snd[zz, :, cols(c)] = total.astype(jnp.bfloat16)
+                partial_out(zz, c).start()
+
+        loop(0, cuts, one)
+
+    def both(d, action):
+        def side(s, carry):
+            zz = z + d * (2 * s - 1)
+            valid = jnp.logical_and(jnp.logical_and(zz >= 0, zz < nz), jnp.logical_or(d > 0, s == 0))
+
+            @pl.when(valid)
+            def _():
+                action(zz, s)
+
+            return carry
+
+        lax.fori_loop(0, 2, side, 0)
+
+    def receive(d, c):
+        def forward(zz, s):
+            hop(zz, c, True).wait_recv()
+
+            @pl.when(jnp.logical_and(zz < z, z + 1 < nz))
+            def _():
+                hop(zz, c, True).start()
+
+            @pl.when(jnp.logical_and(zz > z, z > 0))
+            def _():
+                hop(zz, c, False).start()
+
+        both(d, forward)
+        both(d, lambda zz, s: pack(zz, c, blk[zz, :, cols(c)]))
+
+    learn(z)
+    loop(0, cuts, lambda c: pack(z, c, normed[:, cols(c)]))
+    for k in range(1, nz):
+        facts_in(k).wait_recv()
+        learn((z - k + nz) % nz)
+    for load in loads:
+        load.wait()
+
+    def turn(d, carry):
+        @pl.when(d < nz)
+        def _():
+            receive(d, 0)
+
+        both(d - 1, lambda zz, s: expert(zz))
+
+        @pl.when(d < nz)
+        def _():
+            loop(1, cuts, lambda c: receive(d, c))
+
+        both(d - 1, lambda zz, s: gather(zz))
+        return carry
+
+    lax.fori_loop(1, nz + 1, turn, 0)
+
+    below = 2 * z < nz - 1
+
+    def relay(level, c):
+        def pass_on(s, carry):
+            upward = jnp.where(below, s == 0, s == 1)
+            zz = jnp.where(upward, level, nz - 1 - level)
+            valid = jnp.where(
+                upward, jnp.logical_and(zz > z, z > 0), jnp.logical_and(zz < z, z < nz - 1)
+            )
+
+            @pl.when(valid)
+            def _():
+                partial_in(zz, c).wait_recv()
+                snd[zz, :, cols(c)] = (
+                    part[zz, :, cols(c)] + inc[zz, :, cols(c)].astype(jnp.float32)
+                ).astype(jnp.bfloat16)
+                partial_out(zz, c).start()
+
+            return carry
+
+        lax.fori_loop(0, 2, pass_on, 0)
+
+    loop(1, nz, lambda level: loop(0, cuts, lambda c: relay(level, c)))
+
+    def finish(c):
+        @pl.when(z > 0)
+        def _():
+            partial_in(nz, c).wait_recv()
+            part[z, :, cols(c)] += inc[nz, :, cols(c)].astype(jnp.float32)
+
+        @pl.when(z + 1 < nz)
+        def _():
+            partial_in(z, c).wait_recv()
+            part[z, :, cols(c)] += inc[z, :, cols(c)].astype(jnp.float32)
+
+        out_ref[:, cols(c)] = (
+            stream[:, cols(c)].astype(jnp.float32) + part[z, :, cols(c)]
+        ).astype(jnp.bfloat16)
+
+    loop(0, cuts, finish)
+
+    for k in range(1, nz):
+        facts(k).wait_send()
+
+    def sent(zz):
+        dispatch_all(zz).wait_send()
+        answer_sent(zz).wait_send()
+
+        def one(c):
+            @pl.when(jnp.logical_and(zz <= z, z + 1 < nz))
+            def _():
+                hop(zz, c, True).wait_send()
+
+            @pl.when(jnp.logical_and(zz >= z, z > 0))
+            def _():
+                hop(zz, c, False).wait_send()
+
+            @pl.when(zz != z)
+            def _():
+                partial_out(zz, c).wait_send()
+
+        loop(0, cuts, one)
+
+    loop(0, nz, sent)
+
+
+def moe(mesh, nz, nx, cap, normed, stream, route, share_w, expert_gate, expert_up, expert_down):
     ntp = mesh.shape["tp"]
-    count = mesh.shape["sp"] * ntp
-    width = outgoing.shape[1]
+    plane = nx * ntp
+    slots = plane * cap
+    toks, width = normed.shape
     ff = expert_gate.shape[2]
+    cuts = max(1, width // 512)
     dma = pltpu.SemaphoreType.DMA
     low = jnp.bfloat16
     return pl.pallas_call(
-        functools.partial(moe_kernel, count, ntp, cap),
+        functools.partial(moe_kernel, nz, nx, ntp, cap, cuts),
         out_shape=jax.ShapeDtypeStruct(stream.shape, low),
         in_specs=[pl.BlockSpec(memory_space=pltpu.VMEM)] * 4
         + [pl.BlockSpec(memory_space=pl.ANY)] * 3,
         out_specs=pl.BlockSpec(memory_space=pltpu.VMEM),
         scratch_shapes=[
-            pltpu.VMEM((count * cap, width), low),
-            pltpu.VMEM((count * cap, width), low),
-            pltpu.VMEM((count * cap, width), low),
-            pltpu.VMEM((count // 4 * cap, ff), low),
+            pltpu.VMEM((nz, 8, toks), jnp.float32),
+            pltpu.VMEM((nz, toks, width), low),
+            pltpu.VMEM((nz, slots, width), low),
+            pltpu.VMEM((nz, slots, width), low),
+            pltpu.VMEM((nz, slots, width), low),
+            pltpu.VMEM((nz, slots, width), low),
+            pltpu.VMEM((nz + 1, toks, width), low),
+            pltpu.VMEM((nz, toks, width), jnp.float32),
+            pltpu.VMEM((nz, toks, width), low),
+            pltpu.VMEM((nz, slots, toks), low),
+            pltpu.VMEM((nz, toks, 2 * slots), low),
+            pltpu.VMEM((slots, ff), low),
             pltpu.VMEM((width, ff), low),
             pltpu.VMEM((width, ff), low),
             pltpu.VMEM((ff, width), low),
-            dma((count,)), dma((count,)), dma((count,)), dma((count,)), dma((3,)),
+            dma((nz,)), dma((nz,)),
+            dma((nz, cuts)), dma((nz, cuts)), dma((nz, cuts)),
+            dma((nz,)), dma((nz,)),
+            dma((nz,)), dma((nz, cuts)),
+            dma((nz, cuts)), dma((nz + 1, cuts)),
+            dma((3,)),
         ],
         compiler_params=pltpu.CompilerParams(
-            collective_id=1, has_side_effects=True, vmem_limit_bytes=60 << 20
+            collective_id=1, has_side_effects=True, vmem_limit_bytes=62 << 20
         ),
         name="moe",
-    )(outgoing, stream, pick, share_w, expert_gate, expert_up, expert_down)
+    )(normed, stream, route, share_w, expert_gate, expert_up, expert_down)
 
 
 def local(
@@ -398,25 +657,12 @@
     normed = (unit_length_rows(stream) * norm_gain).astype(jnp.bfloat16)
     row_count = normed.shape[0]
     top_count = route_expert.shape[1]
-    experts = lax.axis_size("sp") * lax.axis_size("tp")
+    n = mesh.shape["sp"]
+    experts = n * mesh.shape["tp"]
     capacity = -(-max(2, 2 * top_count * row_count // experts) // 16) * 16
-    flat_expert = route_expert.reshape(-1)
-    onehot = (flat_expert[:, None] == jnp.arange(experts, dtype=jnp.int32)[None, :]).astype(
-        jnp.int32
-    )
-    earlier = jnp.cumsum(onehot, axis=0) - onehot
-    slot_rank = jnp.sum(earlier * onehot, axis=1)
-    me = lax.axis_index("sp") * lax.axis_size("tp") + lax.axis_index("tp")
-    target = ((flat_expert - me + experts) % experts) * capacity + slot_rank
-    placing = jnp.arange(experts * capacity, dtype=jnp.int32)[:, None] == target[None, :]
-    placing = jnp.any(placing.reshape(experts * capacity, row_count, top_count), axis=2).astype(
-        jnp.bfloat16
-    )
-    outgoing = jnp.dot(placing, normed, preferred_element_type=jnp.float32).astype(jnp.bfloat16)
-    places = jnp.arange(experts * capacity, dtype=jnp.int32)
-    pick = target.reshape(row_count, top_count).T[:, :, None] == places
+    nz, nx = ring_sizes(mesh, n)
     return moe(
-        mesh, capacity, outgoing, stream, pick.astype(jnp.bfloat16), route_weight,
+        mesh, nz, nx, capacity, normed, stream, route_expert.T, route_weight.T,
         expert_gate, expert_up, expert_down,
     )
 

time: 152 us -> 138 us (0.908)
  the two profiles are of different devices: /device:TPU:16 before, /device:TPU:0 now
where the time goes in v1:
time: 138 us; the launch traced here: 137 us
  Pallas kernels  127 us (92%)
  local copies, waits for them, and re-layouts  4.73 us (3%)
  matrix products  2.99 us (2%)
  other arithmetic  2.53 us (2%)
    pallas_call x1, Pallas kernels, moe(): pl.pallas_call(functools.partial(moe_kernel, nz, nx, ntp, cap, cuts), out...  95.4 us
    pallas_call x1, Pallas kernels, attend(): pl.pallas_call(functools.partial(attend_kernel, n, nz, nx, ntp, group), o...  31.6 us
    unnamed x15, local copies, waits for them, and re-layouts  4.65 us
    dot_general x1, matrix products, local(): mixed = jnp.dot(by_token, out_weight, preferred_element_type=jnp.float32)  2.99 us

profile of v1, /device:TPU:0, one launch (start us, length us, event | category | flops | bytes accessed | tf_op | source)
XLA Modules:
  0.0 137.3 jit_solution(1334009316911033414)
XLA Ops:
  0.0 0.0 copy-start.5
  0.0 0.0 copy-start.4
  0.1 0.1 mul.52
  0.2 0.1 select_convert_fusion.ones_ref
  0.3 1.0 fusion.3
  1.3 0.0 copy-start
  1.3 0.9 copy-done
  2.2 0.0 copy-start.1
  2.2 0.9 copy-done.1
  3.2 0.0 copy-start.2
  3.2 0.9 copy-done.2
  4.1 0.0 copy-start.6
  4.1 31.6 %attend.1 = bf16[128,1024]{1,0:T(8,128)(2,1)S(1)} custom-call(bf16[512,256]{1,0:T(8,128)(2,1)S(1)} %copy-done, bf16[512,128]{1,0:T(8,128)(2,1)S(1)} %copy-done.1, bf16[512,128]{1,0:T(8,128)(2,1)S(1)} %copy-done.2, f32[512,128]{1,0:T(8,128)S(1)} %get-tuple-element.8.cos_ref, f32[512,128]{1,0:T(8,128)S(1)} %get-tuple-element.7.sin_ref, ...), custom_call_target="tpu_custom_call" | custom-call | tf_op jit(solution)/shard_map/attend/pallas_call | solution.py:225
  35.6 3.0 %multiply_reduce_fusion = (f32[128]{0:T(128)S(1)}, f32[128,2048]{1,0:T(8,128)S(1)}) fusion(bf16[128,1024]{1,0:T(8,128)(2,1)S(1)} %attend.1, bf16[1024,2048]{1,0:T(8,128)(2,1)} %param.16), kind=kOutput, calls=%fused_computation.6 | convolution fusion | flops 537395072 | bytes 5505536 | tf_op jit(solution)/shard_map/dot_general | solution.py:653
  38.6 0.0 copy-done.5
  38.7 0.0 copy-done.4
  38.7 0.4 fusion
  39.1 0.0 copy-start.3
  39.1 0.0 copy-done.6
  39.1 1.0 fusion.2.normed
  40.1 0.0 copy-done.3
  40.1 95.4 %moe.1 = bf16[128,2048]{1,0:T(8,128)(2,1)} custom-call(bf16[128,2048]{1,0:T(8,128)(2,1)} %fusion.2.normed, bf16[128,2048]{1,0:T(8,128)(2,1)} %copy-done.3, s32[2,128]{1,0:T(2,128)} %bitcast.4, f32[2,128]{1,0:T(2,128)} %bitcast.5, bf16[1,2048,1024]{2,1,0:T(8,128)(2,1)} %gate_hbm.1, bf16[1,2048,1024]{2,1,0:T(8,128)(2,1)} %up_hbm.1, bf16[1,1024,2048]{2,1,0:T(8,128)(2,1)} %down_hbm.1), custom_call_target="tpu_custom_call" | custom-call | tf_op jit(solution)/shard_map/moe/pallas_call | solution.py:601
  135.4 1.9 %copy.14 = bf16[128,2048]{1,0:T(8,128)(2,1)} copy(bf16[128,2048]{1,0:T(8,128)(2,1)} %moe.1) | data formatting | bytes 1048576
  (10 shorter events, 0.1 us)
Async XLA Ops:
  0.0 38.7 %copy-start.5 = (f32[2048]{0:T(1024)S(1)}, f32[2048]{0:T(1024)}, u32[]{:S(2)}) copy-start(f32[2048]{0:T(1024)} %param.17) | copy-start | bytes 24580
  0.0 38.7 %copy-start.4 = (bf16[128,2048]{1,0:T(8,128)(2,1)S(1)}, bf16[128,2048]{1,0:T(8,128)(2,1)}, u32[]{:S(2)}) copy-start(bf16[128,2048]{1,0:T(8,128)(2,1)} %param.15) | copy-start | bytes 1572868
  1.3 1.0 copy-start
  2.2 0.9 copy-start.1
  3.2 0.9 copy-start.2
  4.1 35.0 %copy-start.6 = (f32[2048]{0:T(1024)S(1)}, f32[2048]{0:T(1024)}, u32[]{:S(2)}) copy-start(f32[2048]{0:T(1024)} %param.18) | copy-start | bytes 24580
  39.1 1.0 copy-start.3

commit v2 on v1

--- a/solution.py
+++ b/solution.py
@@ -245,7 +245,7 @@
 
 
 def moe_kernel(
-    nz, nx, ntp, cap, cuts,
+    nz, nx, ntp, cap, cuts, pieces,
     normed, stream, route, share_w, gate_hbm, up_hbm, down_hbm,
     out_ref,
     info, blk, tx, rx, res, ret, inc, part, snd, place, weigh, act, gate, up, down,
@@ -259,13 +259,20 @@
     slots = plane * cap
     toks, width = normed.shape
     wide = width // cuts
+    fine = width // pieces
     others = (plane - 1) * cap
 
     def device(zz, pp):
         return (zz * nx + pp // ntp, pp % ntp)
 
+    peers = [(p + q) % plane for q in range(plane)]
+    homes = [device(z, pp) for pp in peers]
+
     def cols(c):
         return pl.ds(pl.multiple_of(c * wide, wide), wide)
+
+    def part_cols(c):
+        return pl.ds(pl.multiple_of(c * fine, fine), fine)
 
     def rows(pp):
         return pl.ds(pl.multiple_of(pp * cap, cap), cap)
@@ -306,10 +313,10 @@
         )
 
     def dispatch(zz, c, q):
-        pp = (p + q) % plane
+        pp = peers[q]
         return remote(
             tx.at[zz, rows(pp), cols(c)], rx.at[zz, rows(p), cols(c)],
-            send_o.at[zz], recv_o.at[zz], device(z, pp),
+            send_o.at[zz], recv_o.at[zz], homes[q],
         )
 
     def dispatch_all(zz):
@@ -317,16 +324,16 @@
         return remote(tx.at[zz, some], rx.at[zz, some], send_o.at[zz], recv_o.at[zz], device(z, p))
 
     def answer(zz, c, q):
-        pp = (p + q) % plane
+        pp = peers[q]
         return remote(
-            res.at[zz, rows(pp), cols(c)], ret.at[zz, rows(p), cols(c)],
-            send_r.at[zz], recv_r.at[zz, c], device(z, pp),
+            res.at[zz, rows(pp), part_cols(c)], ret.at[zz, rows(p), part_cols(c)],
+            send_r.at[zz], recv_r.at[zz, c], homes[q],
         )
 
     def answer_in(zz, c):
         some = pl.ds(0, others)
         return remote(
-            res.at[zz, some, cols(c)], ret.at[zz, some, cols(c)],
+            res.at[zz, some, part_cols(c)], ret.at[zz, some, part_cols(c)],
             send_r.at[zz], recv_r.at[zz, c], device(z, p),
         )
 
@@ -334,17 +341,19 @@
         some = pl.ds(0, others)
         return remote(res.at[zz, some], ret.at[zz, some], send_r.at[zz], recv_r.at[zz, 0], device(z, p))
 
+    def starts(zz):
+        return jnp.where(zz > z, z == 0, z == nz - 1)
+
     def partial_out(zz, c):
-        step = jnp.where(zz > z, 1, -1)
         slot = jnp.where(zz == z + 1, nz, zz)
         return remote(
-            snd.at[zz, :, cols(c)], inc.at[slot, :, cols(c)],
-            send_p.at[zz, c], recv_p.at[slot, c], device(z + step, p),
+            snd.at[zz, :, part_cols(c)], inc.at[slot, :, part_cols(c)],
+            send_p.at[zz, c], recv_p.at[slot, c], device(z + jnp.where(zz > z, 1, -1), p),
         )
 
     def partial_in(slot, c):
         return remote(
-            snd.at[0, :, cols(c)], inc.at[slot, :, cols(c)],
+            snd.at[0, :, part_cols(c)], inc.at[slot, :, part_cols(c)],
             send_p.at[0, c], recv_p.at[slot, c], device(z, p),
         )
 
@@ -413,8 +422,8 @@
             dispatch(zz, c, q).start()
         rx[zz, rows(p), cols(c)] = tx[zz, rows(p), cols(c)]
 
-    def columns(first, total, body):
-        tile = math.gcd(total, 256)
+    def columns(first, total, most, body):
+        tile = math.gcd(total, most)
 
         def one(c, carry):
             body(pl.ds(pl.multiple_of(first + c * tile, tile), tile))
@@ -436,40 +445,30 @@
                 act[...], down[:, at], preferred_element_type=jnp.float32
             ).astype(jnp.bfloat16)
 
-        columns(0, gate.shape[1], hidden)
+        columns(0, gate.shape[1], max(256, min(1024, 131072 // slots)), hidden)
 
         def send(c):
-            columns(c * wide, wide, project)
+            columns(c * fine, fine, 512, project)
             for q in range(1, plane):
                 answer(zz, c, q).start()
-            ret[zz, rows(p), cols(c)] = res[zz, rows(p), cols(c)]
-
-        loop(0, cuts, send)
-
-    def gather(zz):
-        last = jnp.logical_and(
-            zz != z,
-            jnp.logical_or(
-                jnp.logical_and(zz > z, z == 0), jnp.logical_and(zz < z, z == nz - 1)
-            ),
-        )
-
-        def one(c):
-            answer_in(zz, c).wait_recv()
-            back = ret[zz, :, cols(c)]
-            total = jnp.dot(
-                weigh[zz, :, 0:slots], back, preferred_element_type=jnp.float32
-            ) + jnp.dot(
-                weigh[zz, :, slots : 2 * slots], back, preferred_element_type=jnp.float32
-            )
-            part[zz, :, cols(c)] = total
-
-            @pl.when(last)
-            def _():
-                snd[zz, :, cols(c)] = total.astype(jnp.bfloat16)
-                partial_out(zz, c).start()
-
-        loop(0, cuts, one)
+            ret[zz, rows(p), part_cols(c)] = res[zz, rows(p), part_cols(c)]
+
+        loop(0, pieces, send)
+
+    def gather(zz, c):
+        answer_in(zz, c).wait_recv()
+        back = ret[zz, :, part_cols(c)]
+        total = jnp.dot(
+            weigh[zz, :, 0:slots], back, preferred_element_type=jnp.float32
+        ) + jnp.dot(
+            weigh[zz, :, slots : 2 * slots], back, preferred_element_type=jnp.float32
+        )
+        part[zz, :, part_cols(c)] = total
+
+        @pl.when(jnp.logical_and(zz != z, starts(zz)))
+        def _():
+            snd[zz, :, part_cols(c)] = total.astype(jnp.bfloat16)
+            partial_out(zz, c).start()
 
     def both(d, action):
         def side(s, carry):
@@ -507,6 +506,31 @@
     for load in loads:
         load.wait()
 
+    below = 2 * z < nz - 1
+    inner = jnp.logical_and(z > 0, z < nz - 1)
+
+    def relay(level, step, lag):
+        def pass_on(s, carry):
+            upward = jnp.where(below, s == 0, s == 1)
+            zz = jnp.where(upward, level, nz - 1 - level)
+            c = step - s * lag
+            valid = jnp.logical_and(
+                jnp.where(upward, zz > z, zz < z), jnp.logical_not(starts(zz))
+            )
+            valid = jnp.logical_and(valid, jnp.logical_and(c >= 0, c < pieces))
+
+            @pl.when(valid)
+            def _():
+                partial_in(zz, c).wait_recv()
+                snd[zz, :, part_cols(c)] = (
+                    part[zz, :, part_cols(c)] + inc[zz, :, part_cols(c)].astype(jnp.float32)
+                ).astype(jnp.bfloat16)
+                partial_out(zz, c).start()
+
+            return carry
+
+        lax.fori_loop(0, 2, pass_on, 0)
+
     def turn(d, carry):
         @pl.when(d < nz)
         def _():
@@ -518,51 +542,35 @@
         def _():
             loop(1, cuts, lambda c: receive(d, c))
 
-        both(d - 1, lambda zz, s: gather(zz))
+        def collect(c):
+            @pl.when(jnp.logical_and(d == nz - 1, inner))
+            def _():
+                loop(1, nz - 1, lambda level: relay(level, c, 0))
+
+            @pl.when(d > 1)
+            def _():
+                both(d - 1, lambda zz, s: gather(zz, c))
+
+        loop(0, pieces, collect)
         return carry
 
     lax.fori_loop(1, nz + 1, turn, 0)
-
-    below = 2 * z < nz - 1
-
-    def relay(level, c):
-        def pass_on(s, carry):
-            upward = jnp.where(below, s == 0, s == 1)
-            zz = jnp.where(upward, level, nz - 1 - level)
-            valid = jnp.where(
-                upward, jnp.logical_and(zz > z, z > 0), jnp.logical_and(zz < z, z < nz - 1)
-            )
-
-            @pl.when(valid)
-            def _():
-                partial_in(zz, c).wait_recv()
-                snd[zz, :, cols(c)] = (
-                    part[zz, :, cols(c)] + inc[zz, :, cols(c)].astype(jnp.float32)
-                ).astype(jnp.bfloat16)
-                partial_out(zz, c).start()
-
-            return carry
-
-        lax.fori_loop(0, 2, pass_on, 0)
-
-    loop(1, nz, lambda level: loop(0, cuts, lambda c: relay(level, c)))
+    loop(0, pieces, lambda c: gather(z, c))
+    loop(0, pieces + 2, lambda c: relay(nz - 1, c, 2))
 
     def finish(c):
-        @pl.when(z > 0)
-        def _():
-            partial_in(nz, c).wait_recv()
-            part[z, :, cols(c)] += inc[nz, :, cols(c)].astype(jnp.float32)
-
-        @pl.when(z + 1 < nz)
-        def _():
-            partial_in(z, c).wait_recv()
-            part[z, :, cols(c)] += inc[z, :, cols(c)].astype(jnp.float32)
-
-        out_ref[:, cols(c)] = (
-            stream[:, cols(c)].astype(jnp.float32) + part[z, :, cols(c)]
+        for slot, there in ((nz, z > 0), (z, z + 1 < nz)):
+
+            @pl.when(there)
+            def _():
+                partial_in(slot, c).wait_recv()
+                part[z, :, part_cols(c)] += inc[slot, :, part_cols(c)].astype(jnp.float32)
+
+        out_ref[:, part_cols(c)] = (
+            stream[:, part_cols(c)].astype(jnp.float32) + part[z, :, part_cols(c)]
         ).astype(jnp.bfloat16)
 
-    loop(0, cuts, finish)
+    loop(0, pieces, finish)
 
     for k in range(1, nz):
         facts(k).wait_send()
@@ -580,11 +588,13 @@
             def _():
                 hop(zz, c, False).wait_send()
 
+        def returned(c):
             @pl.when(zz != z)
             def _():
                 partial_out(zz, c).wait_send()
 
         loop(0, cuts, one)
+        loop(0, pieces, returned)
 
     loop(0, nz, sent)
 
@@ -595,11 +605,12 @@
     slots = plane * cap
     toks, width = normed.shape
     ff = expert_gate.shape[2]
-    cuts = max(1, width // 512)
+    cuts = max(1, width // 1024)
+    pieces = max(1, width // 512)
     dma = pltpu.SemaphoreType.DMA
     low = jnp.bfloat16
     return pl.pallas_call(
-        functools.partial(moe_kernel, nz, nx, ntp, cap, cuts),
+        functools.partial(moe_kernel, nz, nx, ntp, cap, cuts, pieces),
         out_shape=jax.ShapeDtypeStruct(stream.shape, low),
         in_specs=[pl.BlockSpec(memory_space=pltpu.VMEM)] * 4
         + [pl.BlockSpec(memory_space=pl.ANY)] * 3,
@@ -623,8 +634,8 @@
             dma((nz,)), dma((nz,)),
             dma((nz, cuts)), dma((nz, cuts)), dma((nz, cuts)),
             dma((nz,)), dma((nz,)),
-            dma((nz,)), dma((nz, cuts)),
-            dma((nz, cuts)), dma((nz + 1, cuts)),
+            dma((nz,)), dma((nz, pieces)),
+            dma((nz, pieces)), dma((nz + 1, pieces)),
             dma((3,)),
         ],
         compiler_params=pltpu.CompilerParams(

time: 138 us -> 124 us (0.90)
  Pallas kernels: 127 us -> 113 us
    pallas_call x1, Pallas kernels: 95.4 us -> 81.8 us  [moe(): pl.pallas_call(functools.partial(moe_kernel, nz, nx, ntp, cap, cuts, piec...]
where the time goes in v2:
time: 124 us
  Pallas kernels  113 us (91%)
  local copies, waits for them, and re-layouts  4.73 us (4%)
  matrix products  2.99 us (2%)
  other arithmetic  2.53 us (2%)
    pallas_call x1, Pallas kernels, moe(): pl.pallas_call(functools.partial(moe_kernel, nz, nx, ntp, cap, cuts, piec...  81.8 us
    pallas_call x1, Pallas kernels, attend(): pl.pallas_call(functools.partial(attend_kernel, n, nz, nx, ntp, group), o...  31.6 us
    unnamed x15, local copies, waits for them, and re-layouts  4.65 us
    dot_general x1, matrix products, local(): mixed = jnp.dot(by_token, out_weight, preferred_element_type=jnp.float32)  2.99 us

profile of v2, /device:TPU:0, one launch (start us, length us, event | category | flops | bytes accessed | tf_op | source)
XLA Modules:
  0.0 123.8 jit_solution(16841470687025488791)
XLA Ops:
  0.0 0.0 copy-start.5
  0.0 0.0 copy-start.4
  0.1 0.1 mul.52
  0.2 0.1 select_convert_fusion.ones_ref
  0.3 1.0 fusion.3
  1.3 0.0 copy-start
  1.3 0.9 copy-done
  2.2 0.0 copy-start.1
  2.2 0.9 copy-done.1
  3.2 0.0 copy-start.2
  3.2 0.9 copy-done.2
  4.1 0.0 copy-start.6
  4.1 31.6 %attend.1 = bf16[128,1024]{1,0:T(8,128)(2,1)S(1)} custom-call(bf16[512,256]{1,0:T(8,128)(2,1)S(1)} %copy-done, bf16[512,128]{1,0:T(8,128)(2,1)S(1)} %copy-done.1, bf16[512,128]{1,0:T(8,128)(2,1)S(1)} %copy-done.2, f32[512,128]{1,0:T(8,128)S(1)} %get-tuple-element.8.cos_ref, f32[512,128]{1,0:T(8,128)S(1)} %get-tuple-element.7.sin_ref, ...), custom_call_target="tpu_custom_call" | custom-call | tf_op jit(solution)/shard_map/attend/pallas_call | solution.py:225
  35.6 3.0 %multiply_reduce_fusion = (f32[128]{0:T(128)S(1)}, f32[128,2048]{1,0:T(8,128)S(1)}) fusion(bf16[128,1024]{1,0:T(8,128)(2,1)S(1)} %attend.1, bf16[1024,2048]{1,0:T(8,128)(2,1)} %param.16), kind=kOutput, calls=%fused_computation.6 | convolution fusion | flops 537395072 | bytes 5505536 | tf_op jit(solution)/shard_map/dot_general | solution.py:664
  38.6 0.0 copy-done.5
  38.7 0.0 copy-done.4
  38.7 0.4 fusion
  39.1 0.0 copy-start.3
  39.1 0.0 copy-done.6
  39.1 1.0 fusion.2.normed
  40.1 0.0 copy-done.3
  40.1 81.8 %moe.1 = bf16[128,2048]{1,0:T(8,128)(2,1)} custom-call(bf16[128,2048]{1,0:T(8,128)(2,1)} %fusion.2.normed, bf16[128,2048]{1,0:T(8,128)(2,1)} %copy-done.3, s32[2,128]{1,0:T(2,128)} %bitcast.4, f32[2,128]{1,0:T(2,128)} %bitcast.5, bf16[1,2048,1024]{2,1,0:T(8,128)(2,1)} %gate_hbm.1, bf16[1,2048,1024]{2,1,0:T(8,128)(2,1)} %up_hbm.1, bf16[1,1024,2048]{2,1,0:T(8,128)(2,1)} %down_hbm.1), custom_call_target="tpu_custom_call" | custom-call | tf_op jit(solution)/shard_map/moe/pallas_call | solution.py:612
  121.9 1.9 %copy.14 = bf16[128,2048]{1,0:T(8,128)(2,1)} copy(bf16[128,2048]{1,0:T(8,128)(2,1)} %moe.1) | data formatting | bytes 1048576
  (10 shorter events, 0.1 us)
Async XLA Ops:
  0.0 38.7 %copy-start.5 = (f32[2048]{0:T(1024)S(1)}, f32[2048]{0:T(1024)}, u32[]{:S(2)}) copy-start(f32[2048]{0:T(1024)} %param.17) | copy-start | bytes 24580
  0.0 38.7 %copy-start.4 = (bf16[128,2048]{1,0:T(8,128)(2,1)S(1)}, bf16[128,2048]{1,0:T(8,128)(2,1)}, u32[]{:S(2)}) copy-start(bf16[128,2048]{1,0:T(8,128)(2,1)} %param.15) | copy-start | bytes 1572868
  1.3 1.0 copy-start
  2.2 0.9 copy-start.1
  3.2 0.9 copy-start.2
  4.1 35.0 %copy-start.6 = (f32[2048]{0:T(1024)S(1)}, f32[2048]{0:T(1024)}, u32[]{:S(2)}) copy-start(f32[2048]{0:T(1024)} %param.18) | copy-start | bytes 24580
  39.1 1.0 copy-start.3

commit v3 on v2

--- a/solution.py
+++ b/solution.py
@@ -38,10 +38,11 @@
 
 def attend_kernel(
     n, nz, nx, ntp, group,
-    q_ref, k_ref, v_ref, cos_ref, sin_ref, swap_ref, ones_ref,
+    q_ref, k_ref, v_ref, cos_ref, sin_ref,
     out_ref,
     qs, acc, fb, bb, att, rx,
     send_f, recv_f, send_b, recv_b, send_t, recv_t,
+    fused=None,
 ):
     sp = lax.axis_index("sp")
     tp = lax.axis_index("tp")
@@ -60,8 +61,32 @@
             barrier, inc=1, device_id=(sp, (tp + d) % ntp), device_id_type=MESH
         )
 
-    cos = cos_ref[...]
-    sin = sin_ref[...]
+    lane = lax.broadcasted_iota(jnp.int32, (LANES, LANES), 1)
+    other = lax.broadcasted_iota(jnp.int32, (LANES, LANES), 0)
+    quarter = HEAD_SIZE // 4
+    first = (lane // quarter) % 2 == 0
+    swap = jnp.where(
+        other == jnp.where(first, lane + quarter, lane - quarter),
+        jnp.where(first, -1.0, 1.0), 0.0,
+    ).astype(jnp.bfloat16)
+    ones = jnp.where(
+        other // HEAD_SIZE == lane // HEAD_SIZE, 1.0 / HEAD_SIZE, 0.0
+    ).astype(jnp.bfloat16)
+    span = math.gcd(toks, GRID_W)
+    on_row = lax.broadcasted_iota(jnp.int32, (span, LANES), 1) % HEAD_SIZE < 2 * quarter
+
+    def spread(table):
+        columns = table[0:span]
+        return jnp.concatenate(
+            [
+                jnp.where(on_row, table[span + i : span + i + 1], columns)
+                for i in range(toks // span)
+            ],
+            axis=0,
+        )
+
+    cos = spread(cos_ref)
+    sin = spread(sin_ref)
     low = lax.broadcasted_iota(jnp.int32, (toks, LANES), 1) < HEAD_SIZE
 
     def prepare(block):
@@ -69,12 +94,16 @@
         square = wide * wide
         hi = square.astype(jnp.bfloat16)
         lo = (square - hi.astype(jnp.float32)).astype(jnp.bfloat16)
-        mean = jnp.dot(hi, ones_ref[...], preferred_element_type=jnp.float32) + jnp.dot(
-            lo, ones_ref[...], preferred_element_type=jnp.float32
-        )
-        partner = jnp.dot(block, swap_ref[...], preferred_element_type=jnp.float32)
+        mean = jnp.dot(hi, ones, preferred_element_type=jnp.float32) + jnp.dot(
+            lo, ones, preferred_element_type=jnp.float32
+        )
+        partner = jnp.dot(block, swap, preferred_element_type=jnp.float32)
         return (wide * cos + partner * sin) * lax.rsqrt(mean + epsilon)
 
+    awaited = 2 + ntp - 1
+    if fused is not None:
+        awaited += fused["greet"]()
+        fused["inputs"](0)
     keys = prepare(k_ref[...]).astype(jnp.bfloat16)
     vals = v_ref[...]
     for c in range(2):
@@ -98,11 +127,15 @@
             device_id=(prv, tp), device_id_type=MESH,
         )
 
-    pl.semaphore_wait(barrier, 2 + ntp - 1)
+    pl.semaphore_wait(barrier, awaited)
+    if fused is not None:
+        fused["share"]()
     for i in range(2):
         forward(i).start()
         backward(i).start()
 
+    if fused is not None:
+        fused["inputs"](1)
     scale = HEAD_SIZE ** (-0.5)
     for t in range(heads // 2):
         ready = prepare(q_ref[:, t * LANES : (t + 1) * LANES]) * scale
@@ -147,6 +180,8 @@
                 )
         return carry
 
+    if fused is not None:
+        fused["learn"]()
     lax.fori_loop(0, steps + 1, one_step, 0)
 
     share = toks // ntp
@@ -170,15 +205,23 @@
 
     for d in range(1, ntp):
         across(d).start()
-    rx[tp] = att[tp]
+    if fused is not None:
+        fused["mix"](tp, att.at[tp], True)
+        for d in range(1, ntp):
+            source = (tp + ntp - d) % ntp
+            across(d).wait_recv()
+            fused["mix"](source, rx.at[source], False)
+        fused["norm"]()
+    else:
+        rx[tp] = att[tp]
+        for d in range(1, ntp):
+            across(d).wait_recv()
+        width = q_ref.shape[1]
+        for p in range(ntp):
+            out_ref[:, p * width : (p + 1) * width] = rx[p]
     for i in range(steps):
         forward(i).wait_send()
         backward(i).wait_send()
-    for d in range(1, ntp):
-        across(d).wait_recv()
-    width = q_ref.shape[1]
-    for p in range(ntp):
-        out_ref[:, p * width : (p + 1) * width] = rx[p]
     for d in range(1, ntp):
         across(d).wait_send()
 
@@ -195,9 +238,7 @@
     return n, 1
 
 
-def attend(mesh, query_proj, projected_keys, projected_values):
-    n, ntp = mesh.shape["sp"], mesh.shape["tp"]
-    nz, nx = ring_sizes(mesh, n)
+def attend_inputs(query_proj, projected_keys, projected_values):
     toks, width = query_proj.shape
     heads = width // HEAD_SIZE
     group = heads // (projected_keys.shape[1] // HEAD_SIZE)
@@ -206,45 +247,37 @@
         projected_keys = jnp.pad(projected_keys, ((0, 0), (0, spare)))
         projected_values = jnp.pad(projected_values, ((0, 0), (0, spare)))
     quarter = HEAD_SIZE // 4
-    places = lax.axis_index("sp") * toks + jnp.arange(toks, dtype=jnp.int32)
+    span = math.gcd(toks, GRID_W)
+    places = lax.axis_index("sp") * toks
     frequency = base_theta ** (-jnp.arange(quarter, dtype=jnp.float32) / quarter)
-    lane = jnp.arange(LANES, dtype=jnp.int32)
-    on_row = (lane % HEAD_SIZE) < 2 * quarter
-    spot = jnp.where(on_row[None, :], (places // GRID_W)[:, None], (places % GRID_W)[:, None])
-    angle = spot.astype(jnp.float32) * jnp.tile(frequency, LANES // quarter)[None, :]
-    first = (lane // quarter) % 2 == 0
-    source = jnp.where(first, lane + quarter, lane - quarter)
-    swap = jnp.where(
-        lane[:, None] == source[None, :], jnp.where(first, -1.0, 1.0)[None, :], 0.0
-    ).astype(jnp.bfloat16)
-    ones = jnp.where(
-        lane[:, None] // HEAD_SIZE == lane[None, :] // HEAD_SIZE, 1.0 / HEAD_SIZE, 0.0
-    ).astype(jnp.bfloat16)
-    share = toks // ntp
-    dma = pltpu.SemaphoreType.DMA
+    starts = places + span * jnp.arange(toks // span, dtype=jnp.int32)
+    spot = jnp.concatenate(
+        [(places % GRID_W) + jnp.arange(span, dtype=jnp.int32), starts // GRID_W]
+    )
+    angle = spot.astype(jnp.float32)[:, None] * jnp.tile(frequency, LANES // quarter)[None, :]
+    return group, projected_keys, projected_values, (jnp.cos(angle), jnp.sin(angle))
+
+
+def attend(mesh, nz, nx, query_proj, projected_keys, projected_values):
+    n, ntp = mesh.shape["sp"], mesh.shape["tp"]
+    toks, width = query_proj.shape
+    group, projected_keys, projected_values, tables = attend_inputs(
+        query_proj, projected_keys, projected_values
+    )
     return pl.pallas_call(
         functools.partial(attend_kernel, n, nz, nx, ntp, group),
-        out_shape=jax.ShapeDtypeStruct((share, ntp * width), jnp.bfloat16),
-        in_specs=[pl.BlockSpec(memory_space=pltpu.VMEM)] * 7,
+        out_shape=jax.ShapeDtypeStruct((toks // ntp, ntp * width), jnp.bfloat16),
+        in_specs=[pl.BlockSpec(memory_space=pltpu.VMEM)] * 5,
         out_specs=pl.BlockSpec(memory_space=pltpu.VMEM),
-        scratch_shapes=[
-            pltpu.VMEM((heads * toks, LANES), jnp.bfloat16),
-            pltpu.VMEM((heads * toks, LANES), jnp.float32),
-            pltpu.VMEM((n + 1, 2, toks // 2, LANES), jnp.bfloat16),
-            pltpu.VMEM((n + 1, 2, toks // 2, LANES), jnp.bfloat16),
-            pltpu.VMEM((ntp, share, width), jnp.bfloat16),
-            pltpu.VMEM((ntp, share, width), jnp.bfloat16),
-            dma((n - 1,)), dma((n - 1,)), dma((n - 1,)), dma((n - 1,)),
-            dma((ntp,)), dma((ntp,)),
-        ],
+        scratch_shapes=attend_scratch(n, ntp, toks, width),
         compiler_params=pltpu.CompilerParams(
             collective_id=0, has_side_effects=True, vmem_limit_bytes=40 << 20
         ),
         name="attend",
-    )(query_proj, projected_keys, projected_values, jnp.cos(angle), jnp.sin(angle), swap, ones)
-
-
-def moe_kernel(
+    )(query_proj, projected_keys, projected_values, *tables)
+
+
+def moe_steps(
     nz, nx, ntp, cap, cuts, pieces,
     normed, stream, route, share_w, gate_hbm, up_hbm, down_hbm,
     out_ref,
@@ -357,47 +390,56 @@
             send_p.at[0, c], recv_p.at[slot, c], device(z, p),
         )
 
-    barrier = pltpu.get_barrier_semaphore()
-    for k in range(1, nz):
-        pl.semaphore_signal(barrier, inc=1, device_id=device((z + k) % nz, p), device_id_type=MESH)
-    for q in range(1, plane):
-        pl.semaphore_signal(barrier, inc=1, device_id=device(z, (p + q) % plane), device_id_type=MESH)
     loads = [
         pltpu.make_async_copy(gate_hbm.at[0], gate, wsem.at[0]),
         pltpu.make_async_copy(up_hbm.at[0], up, wsem.at[1]),
         pltpu.make_async_copy(down_hbm.at[0], down, wsem.at[2]),
     ]
-    for load in loads:
-        load.start()
-
-    experts = nz * plane
-    at_expert = lax.broadcasted_iota(jnp.int32, (experts, toks), 0)
-    named = [at_expert == route[k : k + 1, :] for k in range(2)]
-    count = (named[0].astype(jnp.float32) + named[1].astype(jnp.float32)).astype(jnp.bfloat16)
-    before = (
-        lax.broadcasted_iota(jnp.int32, (toks, toks), 0)
-        < lax.broadcasted_iota(jnp.int32, (toks, toks), 1)
-    ).astype(jnp.float32).astype(jnp.bfloat16)
-    earlier = jnp.dot(count, before, preferred_element_type=jnp.float32)
-    lines = []
-    for k in range(2):
-        rank = jnp.sum(jnp.where(named[k], earlier, 0.0), axis=0, keepdims=True)
-        lines.append(route[k : k + 1, :].astype(jnp.float32) * float(cap) + rank)
-    info[z] = jnp.concatenate(
-        lines + [share_w[...], jnp.zeros((4, toks), jnp.float32)], axis=0
-    )
-
-    pl.semaphore_wait(barrier, nz - 1 + plane - 1)
-    for k in range(1, nz):
-        facts(k).start()
-
-    @pl.when(z + 1 < nz)
-    def _():
-        loop(0, cuts, lambda c: own_hop(c, True).start())
-
-    @pl.when(z > 0)
-    def _():
-        loop(0, cuts, lambda c: own_hop(c, False).start())
+
+    def greet():
+        barrier = pltpu.get_barrier_semaphore()
+        for k in range(1, nz):
+            pl.semaphore_signal(
+                barrier, inc=1, device_id=device((z + k) % nz, p), device_id_type=MESH
+            )
+        for q in range(1, plane):
+            pl.semaphore_signal(barrier, inc=1, device_id=homes[q], device_id_type=MESH)
+        return nz - 1 + plane - 1
+
+    def fetch():
+        for load in loads:
+            load.start()
+
+    def own_facts():
+        experts = nz * plane
+        at_expert = lax.broadcasted_iota(jnp.int32, (experts, toks), 0)
+        named = [at_expert == route[k : k + 1, :] for k in range(2)]
+        count = (named[0].astype(jnp.float32) + named[1].astype(jnp.float32)).astype(jnp.bfloat16)
+        before = (
+            lax.broadcasted_iota(jnp.int32, (toks, toks), 0)
+            < lax.broadcasted_iota(jnp.int32, (toks, toks), 1)
+        ).astype(jnp.float32).astype(jnp.bfloat16)
+        earlier = jnp.dot(count, before, preferred_element_type=jnp.float32)
+        lines = []
+        for k in range(2):
+            rank = jnp.sum(jnp.where(named[k], earlier, 0.0), axis=0, keepdims=True)
+            lines.append(route[k : k + 1, :].astype(jnp.float32) * float(cap) + rank)
+        info[z] = jnp.concatenate(
+            lines + [share_w[...], jnp.zeros((4, toks), jnp.float32)], axis=0
+        )
+
+    def share_facts():
+        for k in range(1, nz):
+            facts(k).start()
+
+    def send_own(c):
+        @pl.when(z + 1 < nz)
+        def _():
+            own_hop(c, True).start()
+
+        @pl.when(z > 0)
+        def _():
+            own_hop(c, False).start()
 
     def learn(zz):
         known = info[zz]
@@ -498,13 +540,13 @@
         both(d, forward)
         both(d, lambda zz, s: pack(zz, c, blk[zz, :, cols(c)]))
 
-    learn(z)
-    loop(0, cuts, lambda c: pack(z, c, normed[:, cols(c)]))
-    for k in range(1, nz):
-        facts_in(k).wait_recv()
-        learn((z - k + nz) % nz)
-    for load in loads:
-        load.wait()
+    def learn_others():
+        for k in range(1, nz):
+            facts_in(k).wait_recv()
+            learn((z - k + nz) % nz)
+
+    def pack_own(c):
+        pack(z, c, normed[:, cols(c)])
 
     below = 2 * z < nz - 1
     inner = jnp.logical_and(z > 0, z < nz - 1)
@@ -536,11 +578,17 @@
         def _():
             receive(d, 0)
 
-        both(d - 1, lambda zz, s: expert(zz))
+        @pl.when(jnp.logical_or(inner, d > 1))
+        def _():
+            both(d - 1, lambda zz, s: expert(zz))
 
         @pl.when(d < nz)
         def _():
             loop(1, cuts, lambda c: receive(d, c))
+
+        @pl.when(jnp.logical_and(d == nz, jnp.logical_not(inner)))
+        def _():
+            expert(z)
 
         def collect(c):
             @pl.when(jnp.logical_and(d == nz - 1, inner))
@@ -552,11 +600,8 @@
                 both(d - 1, lambda zz, s: gather(zz, c))
 
         loop(0, pieces, collect)
+
         return carry
-
-    lax.fori_loop(1, nz + 1, turn, 0)
-    loop(0, pieces, lambda c: gather(z, c))
-    loop(0, pieces + 2, lambda c: relay(nz - 1, c, 2))
 
     def finish(c):
         for slot, there in ((nz, z > 0), (z, z + 1 < nz)):
@@ -570,11 +615,6 @@
             stream[:, part_cols(c)].astype(jnp.float32) + part[z, :, part_cols(c)]
         ).astype(jnp.bfloat16)
 
-    loop(0, pieces, finish)
-
-    for k in range(1, nz):
-        facts(k).wait_send()
-
     def sent(zz):
         dispatch_all(zz).wait_send()
         answer_sent(zz).wait_send()
@@ -596,53 +636,242 @@
         loop(0, cuts, one)
         loop(0, pieces, returned)
 
-    loop(0, nz, sent)
+    def run():
+        for load in loads:
+            load.wait()
+        lax.fori_loop(1, nz + 1, turn, 0)
+        loop(0, pieces, lambda c: gather(z, c))
+        loop(0, pieces + 2, lambda c: relay(nz - 1, c, 2))
+        loop(0, pieces, finish)
+
+        for k in range(1, nz):
+            facts(k).wait_send()
+        loop(0, nz, sent)
+
+    return dict(
+        greet=greet, fetch=fetch, own_facts=own_facts, share_facts=share_facts, learn=learn,
+        learn_others=learn_others, send_own=send_own, pack_own=pack_own, run=run, place=z,
+    )
+
+
+def moe_kernel(nz, nx, ntp, cap, cuts, pieces, *refs):
+    steps = moe_steps(nz, nx, ntp, cap, cuts, pieces, *refs)
+    awaited = steps["greet"]()
+    steps["fetch"]()
+    steps["own_facts"]()
+    pl.semaphore_wait(pltpu.get_barrier_semaphore(), awaited)
+    steps["share_facts"]()
+    for c in range(cuts):
+        steps["send_own"](c)
+    steps["learn"](steps["place"])
+    for c in range(cuts):
+        steps["pack_own"](c)
+    steps["learn_others"]()
+    steps["run"]()
+
+
+def layer_kernel(n, nz, nx, ntp, group, cap, cuts, pieces, parts, *refs):
+    (
+        q_hbm, k_hbm, v_hbm, residual_hbm, mixer_hbm, cos, sin,
+        mix_gain, norm_gain, route, share_w, gate_hbm, up_hbm, down_hbm, out_ref,
+        q, k, v, residual, mixer, normed, stream, insem,
+    ) = refs[:23]
+    attend_refs = refs[23 : 23 + parts]
+    moe_refs = refs[23 + parts :]
+    mixed = moe_refs[7].at[0]
+    copies = [
+        pltpu.make_async_copy(src, dst, insem.at[i])
+        for i, (src, dst) in enumerate(
+            ((k_hbm, k), (v_hbm, v), (q_hbm, q), (residual_hbm, residual), (mixer_hbm, mixer))
+        )
+    ]
+    for copy in copies:
+        copy.start()
+    steps = moe_steps(
+        nz, nx, ntp, cap, cuts, pieces,
+        normed, stream, route, share_w, gate_hbm, up_hbm, down_hbm, out_ref, *moe_refs,
+    )
+
+    def inputs(stage):
+        for copy in copies[:2] if stage == 0 else copies[2:3]:
+            copy.wait()
+
+    def greet():
+        awaited = steps["greet"]()
+        steps["fetch"]()
+        steps["own_facts"]()
+        return awaited
+
+    def learn():
+        steps["learn"](steps["place"])
+        steps["learn_others"]()
+
+    toks, width = normed.shape
+    depth = q.shape[1]
+    tile = width // cuts
+
+    def each(action):
+        for c in range(cuts):
+            action(c, slice(c * tile, (c + 1) * tile))
+
+    def mix(source, block, first):
+        if first:
+            for copy in copies[3:]:
+                copy.wait()
+        rows = pl.ds(pl.multiple_of(source * depth, depth), depth)
+
+        def one(c, at):
+            term = jnp.dot(block[...], mixer[rows, at], preferred_element_type=jnp.float32)
+            mixed[:, at] = term if first else mixed[:, at] + term
+
+        each(one)
+
+    def norm():
+        def squares(values):
+            return jnp.sum(values * values, axis=-1, keepdims=True)
+
+        total = jnp.zeros((toks, 1), jnp.float32)
+        for c in range(cuts):
+            total += squares(mixed[:, c * tile : (c + 1) * tile])
+        scale = lax.rsqrt(total / width + epsilon)
+        total = jnp.zeros((toks, 1), jnp.float32)
+        for c in range(cuts):
+            at = slice(c * tile, (c + 1) * tile)
+            row = (
+                residual[:, at].astype(jnp.float32) + mixed[:, at] * scale * mix_gain[:, at]
+            ).astype(jnp.bfloat16)
+            stream[:, at] = row
+            total += squares(row.astype(jnp.float32))
+        scale = lax.rsqrt(total / width + epsilon)
+        for c in range(cuts):
+            at = slice(c * tile, (c + 1) * tile)
+            normed[:, at] = (
+                stream[:, at].astype(jnp.float32) * scale * norm_gain[:, at]
+            ).astype(jnp.bfloat16)
+            steps["send_own"](c)
+        for c in range(cuts):
+            steps["pack_own"](c)
+
+    attend_kernel(
+        n, nz, nx, ntp, group, q, k, v, cos, sin, None, *attend_refs,
+        fused=dict(
+            greet=greet, inputs=inputs, share=steps["share_facts"], learn=learn, mix=mix, norm=norm
+        ),
+    )
+    steps["run"]()
+
+
+def attend_scratch(n, ntp, toks, width):
+    heads = width // HEAD_SIZE
+    share = toks // ntp
+    dma = pltpu.SemaphoreType.DMA
+    return [
+        pltpu.VMEM((heads * toks, LANES), jnp.bfloat16),
+        pltpu.VMEM((heads * toks, LANES), jnp.float32),
+        pltpu.VMEM((n + 1, 2, toks // 2, LANES), jnp.bfloat16),
+        pltpu.VMEM((n + 1, 2, toks // 2, LANES), jnp.bfloat16),
+        pltpu.VMEM((ntp, share, width), jnp.bfloat16),
+        pltpu.VMEM((ntp, share, width), jnp.bfloat16),
+        dma((n - 1,)), dma((n - 1,)), dma((n - 1,)), dma((n - 1,)),
+        dma((ntp,)), dma((ntp,)),
+    ]
+
+
+def moe_scratch(nz, slots, toks, width, ff, cuts, pieces):
+    dma = pltpu.SemaphoreType.DMA
+    low = jnp.bfloat16
+    return [
+        pltpu.VMEM((nz, 8, toks), jnp.float32),
+        pltpu.VMEM((nz, toks, width), low),
+        pltpu.VMEM((nz, slots, width), low),
+        pltpu.VMEM((nz, slots, width), low),
+        pltpu.VMEM((nz, slots, width), low),
+        pltpu.VMEM((nz, slots, width), low),
+        pltpu.VMEM((nz + 1, toks, width), low),
+        pltpu.VMEM((nz, toks, width), jnp.float32),
+        pltpu.VMEM((nz, toks, width), low),
+        pltpu.VMEM((nz, slots, toks), low),
+        pltpu.VMEM((nz, toks, 2 * slots), low),
+        pltpu.VMEM((slots, ff), low),
+        pltpu.VMEM((width, ff), low),
+        pltpu.VMEM((width, ff), low),
+        pltpu.VMEM((ff, width), low),
+        dma((nz,)), dma((nz,)),
+        dma((nz, cuts)), dma((nz, cuts)), dma((nz, cuts)),
+        dma((nz,)), dma((nz,)),
+        dma((nz,)), dma((nz, pieces)),
+        dma((nz, pieces)), dma((nz + 1, pieces)),
+        dma((3,)),
+    ]
 
 
 def moe(mesh, nz, nx, cap, normed, stream, route, share_w, expert_gate, expert_up, expert_down):
     ntp = mesh.shape["tp"]
-    plane = nx * ntp
-    slots = plane * cap
+    slots = nx * ntp * cap
     toks, width = normed.shape
     ff = expert_gate.shape[2]
     cuts = max(1, width // 1024)
     pieces = max(1, width // 512)
-    dma = pltpu.SemaphoreType.DMA
-    low = jnp.bfloat16
     return pl.pallas_call(
         functools.partial(moe_kernel, nz, nx, ntp, cap, cuts, pieces),
-        out_shape=jax.ShapeDtypeStruct(stream.shape, low),
+        out_shape=jax.ShapeDtypeStruct(stream.shape, jnp.bfloat16),
         in_specs=[pl.BlockSpec(memory_space=pltpu.VMEM)] * 4
         + [pl.BlockSpec(memory_space=pl.ANY)] * 3,
         out_specs=pl.BlockSpec(memory_space=pltpu.VMEM),
-        scratch_shapes=[
-            pltpu.VMEM((nz, 8, toks), jnp.float32),
-            pltpu.VMEM((nz, toks, width), low),
-            pltpu.VMEM((nz, slots, width), low),
-            pltpu.VMEM((nz, slots, width), low),
-            pltpu.VMEM((nz, slots, width), low),
-            pltpu.VMEM((nz, slots, width), low),
-            pltpu.VMEM((nz + 1, toks, width), low),
-            pltpu.VMEM((nz, toks, width), jnp.float32),
-            pltpu.VMEM((nz, toks, width), low),
-            pltpu.VMEM((nz, slots, toks), low),
-            pltpu.VMEM((nz, toks, 2 * slots), low),
-            pltpu.VMEM((slots, ff), low),
-            pltpu.VMEM((width, ff), low),
-            pltpu.VMEM((width, ff), low),
-            pltpu.VMEM((ff, width), low),
-            dma((nz,)), dma((nz,)),
-            dma((nz, cuts)), dma((nz, cuts)), dma((nz, cuts)),
-            dma((nz,)), dma((nz,)),
-            dma((nz,)), dma((nz, pieces)),
-            dma((nz, pieces)), dma((nz + 1, pieces)),
-            dma((3,)),
-        ],
+        scratch_shapes=moe_scratch(nz, slots, toks, width, ff, cuts, pieces),
         compiler_params=pltpu.CompilerParams(
             collective_id=1, has_side_effects=True, vmem_limit_bytes=62 << 20
         ),
         name="moe",
     )(normed, stream, route, share_w, expert_gate, expert_up, expert_down)
+
+
+def layer(
+    mesh, nz, nx, cap, query_proj, projected_keys, projected_values, residual, out_weight,
+    mix_gain, norm_gain, route, share_w, expert_gate, expert_up, expert_down,
+):
+    n, ntp = mesh.shape["sp"], mesh.shape["tp"]
+    slots = nx * ntp * cap
+    group, projected_keys, projected_values, tables = attend_inputs(
+        query_proj, projected_keys, projected_values
+    )
+    toks, depth = query_proj.shape
+    rows, width = residual.shape
+    ff = expert_gate.shape[2]
+    cuts = max(1, width // 1024)
+    pieces = max(1, width // 512)
+    low = jnp.bfloat16
+    inner = attend_scratch(n, ntp, toks, depth)
+    vmem = pl.BlockSpec(memory_space=pltpu.VMEM)
+    anywhere = pl.BlockSpec(memory_space=pl.ANY)
+    return pl.pallas_call(
+        functools.partial(
+            layer_kernel, n, nz, nx, ntp, group, cap, cuts, pieces, len(inner)
+        ),
+        out_shape=jax.ShapeDtypeStruct(residual.shape, low),
+        in_specs=[anywhere] * 5 + [vmem] * 6 + [anywhere] * 3,
+        out_specs=vmem,
+        scratch_shapes=[
+            pltpu.VMEM((toks, depth), low),
+            pltpu.VMEM(projected_keys.shape, low),
+            pltpu.VMEM(projected_values.shape, low),
+            pltpu.VMEM((rows, width), low),
+            pltpu.VMEM(out_weight.shape, low),
+            pltpu.VMEM((rows, width), low),
+            pltpu.VMEM((rows, width), low),
+            pltpu.SemaphoreType.DMA((5,)),
+        ]
+        + inner
+        + moe_scratch(nz, slots, rows, width, ff, cuts, pieces),
+        compiler_params=pltpu.CompilerParams(
+            collective_id=2, has_side_effects=True, vmem_limit_bytes=62 << 20
+        ),
+        name="layer",
+    )(
+        query_proj, projected_keys, projected_values, residual, out_weight, *tables,
+        mix_gain[None, :], norm_gain[None, :], route, share_w,
+        expert_gate, expert_up, expert_down,
+    )
 
 
 def local(
@@ -660,18 +889,24 @@
     expert_up,
     expert_down,
 ):
-    by_token = attend(mesh, query_proj, projected_keys, projected_values)
+    row_count = residual.shape[0]
+    top_count = route_expert.shape[1]
+    n, ntp = mesh.shape["sp"], mesh.shape["tp"]
+    experts = n * ntp
+    capacity = -(-max(2, 2 * top_count * row_count // experts) // 16) * 16
+    nz, nx = ring_sizes(mesh, n)
+    if nx * ntp * capacity <= 128:
+        return layer(
+            mesh, nz, nx, capacity, query_proj, projected_keys, projected_values, residual,
+            out_weight, mix_gain, norm_gain, route_expert.T, route_weight.T,
+            expert_gate, expert_up, expert_down,
+        )
+    by_token = attend(mesh, nz, nx, query_proj, projected_keys, projected_values)
     mixed = jnp.dot(by_token, out_weight, preferred_element_type=jnp.float32)
     stream = (residual.astype(jnp.float32) + unit_length_rows(mixed) * mix_gain).astype(
         jnp.bfloat16
     )
     normed = (unit_length_rows(stream) * norm_gain).astype(jnp.bfloat16)
-    row_count = normed.shape[0]
-    top_count = route_expert.shape[1]
-    n = mesh.shape["sp"]
-    experts = n * mesh.shape["tp"]
-    capacity = -(-max(2, 2 * top_count * row_count // experts) // 16) * 16
-    nz, nx = ring_sizes(mesh, n)
     return moe(
         mesh, nz, nx, capacity, normed, stream, route_expert.T, route_weight.T,
         expert_gate, expert_up, expert_down,

time: 124 us -> 116 us (0.935)
  matrix products: 2.99 us -> 0 us
  local copies, waits for them, and re-layouts: 4.73 us -> 1.97 us
  other arithmetic: 2.53 us -> 0.95 us
    dot_general x1 -> x0, matrix products: 2.99 us -> none  [local(): mixed = jnp.dot(by_token, out_weight, preferred_element_type=jnp.float32)]
    unnamed x15 -> x1, local copies, waits for them, and re-layouts: 4.65 us -> 1.88 us
    pallas_call x2 -> x1, Pallas kernels: 113 us -> 113 us  [layer(): pl.pallas_call(functools.partial(layer_kernel, n, nz, nx, ntp, group, cap...]
where the time goes in v3:
time: 116 us
  Pallas kernels  113 us (97%)
  local copies, waits for them, and re-layouts  1.97 us (2%)
    pallas_call x1, Pallas kernels, layer(): pl.pallas_call(functools.partial(layer_kernel, n, nz, nx, ntp, group, cap...  113 us

profile of v3, /device:TPU:0, one launch (start us, length us, event | category | flops | bytes accessed | tf_op | source)
XLA Modules:
  0.0 116.2 jit_solution(8046357081237995297)
XLA Ops:
  0.0 0.1 add_convert_fusion
  0.1 0.1 mul.26
  0.2 0.8 multiply_sine_fusion
  1.0 113.3 %layer.1 = bf16[128,2048]{1,0:T(8,128)(2,1)} custom-call(bf16[512,256]{1,0:T(8,128)(2,1)} %refs_0_.1, bf16[512,128]{1,0:T(8,128)(2,1)} %refs_1_.1, bf16[512,128]{1,0:T(8,128)(2,1)} %refs_2_.1, bf16[128,2048]{1,0:T(8,128)(2,1)} %refs_3_.1, bf16[1024,2048]{1,0:T(8,128)(2,1)} %refs_4_.1, f32[72,128]{1,0:T(8,128)} %get-tuple-element.6.refs_5_, ...), custom_call_target="tpu_custom_call" | custom-call | tf_op jit(solution)/shard_map/layer/pallas_call | solution.py:847
  114.4 1.9 %copy.14 = bf16[128,2048]{1,0:T(8,128)(2,1)} copy(bf16[128,2048]{1,0:T(8,128)(2,1)} %layer.1) | data formatting | bytes 1048576
  (4 shorter events, 0.0 us)

commit v4 on v3

--- a/solution.py
+++ b/solution.py
@@ -578,6 +578,10 @@
         def _():
             receive(d, 0)
 
+        @pl.when(jnp.logical_and(d == nz - 1, inner))
+        def _():
+            loop(1, nz - 1, lambda level: relay(level, 0, 0))
+
         @pl.when(jnp.logical_or(inner, d > 1))
         def _():
             both(d - 1, lambda zz, s: expert(zz))
@@ -593,7 +597,10 @@
         def collect(c):
             @pl.when(jnp.logical_and(d == nz - 1, inner))
             def _():
-                loop(1, nz - 1, lambda level: relay(level, c, 0))
+                def ahead(step):
+                    loop(1, nz - 1, lambda level: relay(level, step, 0))
+
+                loop(c + 1, c + 2, ahead)
 
             @pl.when(d > 1)
             def _():

time: 116 us -> 114 us (0.983)
  Pallas kernels: 113 us -> 111 us
    pallas_call x1, Pallas kernels: 113 us -> 111 us  [layer(): pl.pallas_call(functools.partial(layer_kernel, n, nz, nx, ntp, group, cap...]
where the time goes in v4:
time: 114 us
  Pallas kernels  111 us (97%)
  local copies, waits for them, and re-layouts  1.97 us (2%)
    pallas_call x1, Pallas kernels, layer(): pl.pallas_call(functools.partial(layer_kernel, n, nz, nx, ntp, group, cap...  111 us

profile of v4, /device:TPU:0, one launch (start us, length us, event | category | flops | bytes accessed | tf_op | source)
XLA Modules:
  0.0 114.0 jit_solution(7061269580706398246)
XLA Ops:
  0.0 0.1 add_convert_fusion
  0.1 0.1 mul.26
  0.2 0.8 multiply_sine_fusion
  1.0 111.1 %layer.1 = bf16[128,2048]{1,0:T(8,128)(2,1)} custom-call(bf16[512,256]{1,0:T(8,128)(2,1)} %refs_0_.1, bf16[512,128]{1,0:T(8,128)(2,1)} %refs_1_.1, bf16[512,128]{1,0:T(8,128)(2,1)} %refs_2_.1, bf16[128,2048]{1,0:T(8,128)(2,1)} %refs_3_.1, bf16[1024,2048]{1,0:T(8,128)(2,1)} %refs_4_.1, f32[72,128]{1,0:T(8,128)} %get-tuple-element.6.refs_5_, ...), custom_call_target="tpu_custom_call" | custom-call | tf_op jit(solution)/shard_map/layer/pallas_call | solution.py:854
  112.1 1.9 %copy.14 = bf16[128,2048]{1,0:T(8,128)(2,1)} copy(bf16[128,2048]{1,0:T(8,128)(2,1)} %layer.1) | data formatting | bytes 1048576
  (4 shorter events, 0.0 us)
